TPU v7x, 512 devices: a whole 4x4x16 slice. The times are simulated.
512 devices in a mesh: fs: 64 (over z, y), tp: 8 (over x, core).
Axes of the slice: x: 4, y: 4, z: 16, core: 2. Of those that a mesh axis runs over, the one named last changes fastest.
Arguments:
- normed_input: bfloat16 [32768, 4096], P('fs', 'tp'), may hold values from -16 to 16
- value_cotangent: bfloat16 [32768, 2048], P('fs', 'tp'), may hold values from -0.005859375 to 0.005859375
- mixer_output: bfloat16 [32768, 2048], P('fs', 'tp'), may hold values from -6 to 6
- output_cotangent: bfloat16 [32768, 4096], P('fs', 'tp'), may hold values from -0.0078125 to 0.0078125
- value_factor: bfloat16 [4096, 128], replicated, may hold values from -0.5 to 0.5
- output_factor: bfloat16 [2048, 128], replicated, may hold values from -0.5 to 0.5
- value_master: float32 [4096, 2048], P('fs', 'tp'), may hold values from -0.09375 to 0.09375
- value_moment: float32 [128, 2048], P(None, 'tp'), may hold values from -6 to 6
- value_second: float32 [128, 2048], P(None, 'tp'), may hold values from 0.0625 to 16, as said below
- output_master: float32 [2048, 4096], P('fs', 'tp'), may hold values from -0.125 to 0.125
- output_moment: float32 [128, 4096], P(None, 'tp'), may hold values from -6 to 6
- output_second: float32 [128, 4096], P(None, 'tp'), may hold values from 0.0625 to 16, as said below
Outputs:
- value_step: float32 [4096, 2048], P('fs', 'tp')
- value_new: float32 [4096, 2048], P('fs', 'tp')
- value_copy: bfloat16 [4096, 2048], P(None, 'tp')
- value_moment_new: float32 [128, 2048], P(None, 'tp')
- value_second_new: float32 [128, 2048], P(None, 'tp')
- output_step: float32 [2048, 4096], P('fs', 'tp')
- output_new: float32 [2048, 4096], P('fs', 'tp')
- output_copy: bfloat16 [2048, 4096], P(None, 'tp')
- output_moment_new: float32 [128, 4096], P(None, 'tp')
- output_second_new: float32 [128, 4096], P(None, 'tp')
Inputs may be any that keep to these rules, and one draw needn't show every extreme that they name: `value_second`: positive, with a scale that differs between groups of columns. `output_second`: positive, with a scale that differs between groups of columns.
All inputs are finite; a program needn't handle non-finite values.
Results may differ from a plain program's by a relative error of at most 0.004.
Values may be sent and summed in bfloat16 or wider, within the bound.
No kernel may reach another device: no remote copies, remote signals or barrier semaphores. Data moves between devices by JAX's collectives and lax.ppermute only.
A program may use at most 64 MiB of HBM per device.

v0:
```python
import jax
import jax.numpy as jnp
from jax import lax
from jax.sharding import Mesh
from jax.sharding import PartitionSpec as P

D = 4096
WIDTH = 2048
R = 128
FS = ("fs_0", "fs_1")


BETA_ONE = 0.8
BETA_TWO = 0.9
EPSILON = 1e-08
STEP_RATE = 0.005
FLOOR = 0.25


def sent_to_all(shard, axis):
    copies = jnp.broadcast_to(shard, (lax.axis_size(axis), *shard.shape))
    return lax.all_to_all(copies, axis, split_axis=0, concat_axis=0, tiled=True)


def taken_together(shard, axis):
    return sent_to_all(shard, axis).astype(jnp.float32).sum(axis=0)


def padded_to(lines, size):
    spare = -lines.shape[0] % size
    if not spare:
        return lines
    return jnp.concatenate([lines, jnp.zeros((spare, *lines.shape[1:]), lines.dtype)])


def own_block(parts, axes, sequence):
    inside = parts.shape[1:]
    parts = parts.reshape(*(lax.axis_size(a) for a in axes), *inside)
    parts = jnp.moveaxis(parts, sequence, range(len(axes))).reshape(-1, *inside)
    for k in sequence:
        parts = lax.psum_scatter(parts, axes[k], scatter_dimension=0, tiled=True)
    return parts[0]


def stacked_from(shard, axes, sequence):
    parts = shard
    for k in sequence:
        parts = lax.all_gather(parts, axes[k])
    done = sequence[::-1]
    back = [done.index(k) for k in range(len(axes))]
    parts = parts.transpose(*back, *range(len(axes), parts.ndim))
    return parts.reshape(-1, *shard.shape)


def sum_by_parts(shard, axes, sequence):
    size, lines = (lax.axis_size(axes), shard.reshape(-1, *shard.shape[1:][-1:]))
    parts = padded_to(lines, size).reshape(size, -1, *lines.shape[1:])
    own = own_block(parts, axes, sequence)
    whole = stacked_from(own, axes, sequence[::-1]).reshape(-1, *lines.shape[1:])
    return whole[: len(lines)].reshape(shard.shape)


def of_everyone(shard, axis):
    everything = sent_to_all(shard, axis)
    return jnp.sum(everything, axis=0)


def in_one(arrays, axis):
    ends = [0]
    for a in arrays:
        ends.append(ends[-1] + a.size)
    running = of_everyone(jnp.concatenate([a.ravel() for a in arrays]), axis)
    return tuple((running[b:e].reshape(a.shape) for a, b, e in zip(arrays, ends, ends[1:])))


def in_order(parts, dim):
    parts = jnp.moveaxis(parts, 0, dim)
    shape = parts.shape
    return parts.reshape(*shape[:dim], shape[dim] * shape[dim + 1], *shape[dim + 2 :])


def gather_packed(arrays, axis, dims):
    flat = jnp.concatenate([a.reshape(-1) for a in arrays])
    lines, at, done = (lax.all_gather(flat, axis), 0, [])
    for a, dim in zip(arrays, dims):
        parts = lines[:, at : at + a.size].reshape(-1, *a.shape)
        done.append(in_order(parts, dim))
        at += a.size
    return tuple(done)


def contract_rows(left, right):
    return lax.dot_general(
        left.astype(jnp.float32),
        right.astype(jnp.float32),
        (((0,), (0,)), ((), ())),
        preferred_element_type=jnp.float32,
        precision=lax.Precision.HIGHEST,
    )


def moments(first, second, projected):
    first_new = BETA_ONE * first + (1.0 - BETA_ONE) * projected
    second_new = BETA_TWO * second + (1.0 - BETA_TWO) * projected * projected
    normalized = first_new / (jnp.sqrt(second_new) + EPSILON)
    return (first_new, second_new, normalized)


def per_device(
    normed_input,
    value_cotangent,
    mixer_output,
    output_cotangent,
    value_factor,
    output_factor,
    value_master,
    value_moment,
    value_second,
    output_master,
    output_moment,
    output_second,
):
    highest = lax.Precision.HIGHEST
    row_index = lax.axis_index(FS)
    column_index = lax.axis_index("tp")
    value_rows = value_master.shape[0]
    output_rows = output_master.shape[0]
    factor_here = lax.dynamic_slice_in_dim(
        value_factor, row_index * value_rows, value_rows, 0
    ).astype(jnp.float32)
    feature_cols = normed_input.shape[1]
    factor_features = lax.dynamic_slice_in_dim(
        value_factor, column_index * feature_cols, feature_cols, 0
    )
    input_partial = jnp.dot(normed_input, factor_features, preferred_element_type=jnp.float32)
    input_reduced = taken_together(input_partial.astype(jnp.bfloat16), "tp").astype(jnp.float32)
    value_partial = contract_rows(input_reduced, value_cotangent)
    head_cols = mixer_output.shape[1]
    factor_heads = lax.dynamic_slice_in_dim(output_factor, column_index * head_cols, head_cols, 0)
    mixer_partial = jnp.dot(mixer_output, factor_heads, preferred_element_type=jnp.float32).astype(
        jnp.bfloat16
    )
    mixer_partial = lax.optimization_barrier(mixer_partial)
    mixer_reduced = (
        taken_together(mixer_partial.astype(jnp.float32).astype(jnp.bfloat16), "tp")
        .astype(jnp.float32)
        .astype(jnp.bfloat16)
    )
    output_partial = contract_rows(mixer_reduced, output_cotangent)
    value_projected, output_projected = (
        sum_by_parts(value_partial, FS, (0, 1)),
        sum_by_parts(output_partial, FS, (0, 1)),
    )
    value_moment_new, value_second_new, value_norm = moments(
        value_moment, value_second, value_projected
    )
    output_moment_new, output_second_new, output_norm = moments(
        output_moment, output_second, output_projected
    )
    value_total, output_total = in_one(
        (jnp.sum(value_norm * value_norm), jnp.sum(output_norm * output_norm)), "tp"
    )
    value_scale = lax.rsqrt(value_total / (R * WIDTH) + FLOOR)
    output_scale = lax.rsqrt(output_total / (R * D) + FLOOR)
    value_step = value_scale * jnp.dot(factor_here, value_norm, precision=highest)
    output_factor_rows = lax.dynamic_slice_in_dim(
        output_factor, row_index * output_rows, output_rows, 0
    ).astype(jnp.float32)
    output_step = output_scale * jnp.dot(output_factor_rows, output_norm, precision=highest)
    value_new = value_master - STEP_RATE * value_step
    output_new = output_master - STEP_RATE * output_step
    value_copy, output_copy = gather_packed(
        (value_new.astype(jnp.bfloat16), output_new.astype(jnp.bfloat16)), FS, (0, 0)
    )
    return (
        value_step,
        value_new,
        value_copy,
        value_moment_new,
        value_second_new,
        output_step,
        output_new,
        output_copy,
        output_moment_new,
        output_second_new,
    )


def solution(mesh):
    finer = Mesh(mesh.devices.reshape(16, 4, mesh.shape["tp"]), ("fs_0", "fs_1", "tp"))
    placed = (
        P(FS, "tp"),
        P(FS, "tp"),
        P(FS, "tp"),
        P(FS, "tp"),
        P(),
        P(),
        P(FS, "tp"),
        P(None, "tp"),
        P(None, "tp"),
        P(FS, "tp"),
        P(None, "tp"),
        P(None, "tp"),
    )
    return jax.shard_map(
        per_device,
        mesh=finer,
        in_specs=placed,
        out_specs=(
            P(FS, "tp"),
            P(FS, "tp"),
            P(None, "tp"),
            P(None, "tp"),
            P(None, "tp"),
            P(FS, "tp"),
            P(FS, "tp"),
            P(None, "tp"),
            P(None, "tp"),
            P(None, "tp"),
        ),
        check_vma=False,
    )
```

profile of v0, /device:TPU:1, one launch (start us, length us, event | category | flops | bytes accessed | tf_op | source)
XLA Modules:
  0.0 465.8 jit_solution(13149735531977660443)
XLA Ops:
  7.2 1.3 fusion.1
  8.7 1.1 broadcast_in_dim.10
  9.8 10.3 %all-to-all-start.1 = ((bf16[8,512,128]{2,1,0:T(8,128)(2,1)}), bf16[8,512,128]{2,1,0:T(8,128)(2,1)S(1)}, u32[]{:S(2)}, u32[]{:S(2)}) async-start(bf16[8,512,128]{2,1,0:T(8,128)(2,1)} %broadcast_in_dim.10), calls=%async_computation.1 | async-start | bytes 2097152 | tf_op jit(solution)/shard_map/all_to_all | solution.py:22
  20.5 14.5 %all-to-all-done.1 = bf16[8,512,128]{2,1,0:T(8,128)(2,1)S(1)} async-done(((bf16[8,512,128]{2,1,0:T(8,128)(2,1)}), bf16[8,512,128]{2,1,0:T(8,128)(2,1)S(1)}, u32[]{:S(2)}, u32[]{:S(2)}) %all-to-all-start.1) | async-done | bytes 1048608 | tf_op jit(solution)/shard_map/all_to_all | solution.py:22
  35.1 1.1 broadcast_in_dim.9
  36.2 4.4 all-to-all-start
  41.0 14.6 %all-to-all-done = bf16[8,512,128]{2,1,0:T(8,128)(2,1)S(1)} async-done(((bf16[8,512,128]{2,1,0:T(8,128)(2,1)}), bf16[8,512,128]{2,1,0:T(8,128)(2,1)S(1)}, u32[]{:S(2)}, u32[]{:S(2)}) %all-to-all-start) | async-done | bytes 1048608 | tf_op jit(solution)/shard_map/all_to_all | solution.py:22
  56.1 0.9 fusion.2
  57.0 1.0 fusion.5
  58.0 1.3 dynamic-slice.2
  59.3 1.3 dynamic-slice
  61.2 123.2 %all-reduce.8.cloned.1.call-done = (f32[64,2,512]{2,0,1:T(8,128)}, f32[64,2,256]{2,0,1:T(8,128)}) async-done(((f32[64,2,512]{2,0,1:T(8,128)}, f32[64,2,256]{2,0,1:T(8,128)}), (f32[64,2,512]{2,0,1:T(8,128)}, f32[64,2,256]{2,0,1:T(8,128)})) %all-reduce.8.cloned.1.call-update) | async-done | bytes 393232
  184.4 0.8 constant_dynamic-slice_fusion.1
  185.1 0.7 constant_dynamic-slice_fusion.3
  185.9 13.3 %all-reduce.5 = (f32[4,2,512]{2,1,0:T(2,128)S(1)}, f32[4,2,256]{2,1,0:T(2,128)S(1)}) all-reduce(f32[4,2,512]{2,1,0:T(2,128)S(1)} %copy.51, f32[4,2,256]{2,1,0:T(2,128)S(1)} %copy.47), channel_id=8, replica_groups=mesh['fs_0'=16,'fs_1'=4,'tp'=8] {'fs_1'}, use_global_device_ids=true, to_apply=%region_6.0.clone | all-reduce | flops 6144 | bytes 49152
  199.1 0.7 constant_dynamic-slice_fusion
  199.8 0.7 constant_dynamic-slice_fusion.2
  200.5 8.1 %all_gather.24 = f32[4,2,256]{2,1,0:T(2,128)S(1)} all-gather(f32[1,2,256]{2,1,0:T(2,128)S(1)} %constant_dynamic-slice_fusion.2), channel_id=1, replica_groups=mesh['fs_0'=16,'fs_1'=4,'tp'=8] {'fs_1'}, dimensions={0}, use_global_device_ids=true | all-gather | bytes 10240 | tf_op jit(solution)/shard_map/all_gather | solution.py:48
  208.6 9.1 %all_gather.27 = f32[4,2,512]{2,1,0:T(2,128)S(1)} all-gather(f32[1,2,512]{2,1,0:T(2,128)S(1)} %constant_dynamic-slice_fusion), channel_id=1, replica_groups=mesh['fs_0'=16,'fs_1'=4,'tp'=8] {'fs_1'}, dimensions={0}, use_global_device_ids=true | all-gather | bytes 20480 | tf_op jit(solution)/shard_map/all_gather | solution.py:48
  217.7 21.7 %all-gather = f32[64,2,256]{2,1,0:T(2,128)S(1)} all-gather(f32[4,2,256]{2,1,0:T(2,128)S(1)} %all_gather.24), channel_id=2, replica_groups=mesh['fs_0'=16,'fs_1'=4,'tp'=8] {'fs_0'}, dimensions={0}, use_global_device_ids=true | all-gather | bytes 139264 | tf_op jit(solution)/shard_map/all_gather | solution.py:48
  239.5 20.5 %all-gather.1 = f32[64,2,512]{2,1,0:T(2,128)S(1)} all-gather(f32[4,2,512]{2,1,0:T(2,128)S(1)} %all_gather.27), channel_id=3, replica_groups=mesh['fs_0'=16,'fs_1'=4,'tp'=8] {'fs_0'}, dimensions={0}, use_global_device_ids=true | all-gather | bytes 278528 | tf_op jit(solution)/shard_map/all_gather | solution.py:48
  260.2 0.7 multiply_reduce_fusion.1
  260.9 0.8 multiply_reduce_fusion
  261.7 1.4 pad_maximum_fusion.1
  263.6 37.4 %all-to-all-start.2 = ((f32[8,1,2]{2,1,0:T(1,128)}), f32[8,1,2]{2,1,0:T(1,128)S(1)}, u32[]{:S(2)}, u32[]{:S(2)}) async-start(f32[8,1,2]{2,1,0:T(1,128)} %broadcast_in_dim.11), calls=%async_computation.2 | async-start | bytes 8192 | tf_op jit(solution)/shard_map/all_to_all | solution.py:22
  301.0 4.5 all-to-all-done.2
  308.5 1.0 convolution_multiply_fusion
  310.9 130.3 %all-gather.5.cloned.1.call-done = bf16[2097152]{0:T(1024)(128)(2,1)} async-done(((bf16[32768]{0:T(1024)(128)(2,1)}), bf16[2097152]{0:T(1024)(128)(2,1)}) %all-gather.5.cloned.1.call-update) | async-done | bytes 4194320 | tf_op jit(solution)/shard_map/all_gather | solution.py:84
  441.2 7.4 %reshape.56 = bf16[64,32768]{1,0:T(8,128)(2,1)} reshape(bf16[2097152]{0:T(1024)(128)(2,1)} %all-gather.5.cloned.1.call-done) | data formatting | bytes 8388608 | tf_op jit(solution)/shard_map/all_gather | solution.py:84
  448.6 3.9 fusion.20
  452.4 4.2 reshape_reshape.15
  456.6 2.3 reshape_reshape.14
  (58 shorter events, 5.1 us)
Async XLA Ops:
  7.2 12.9 %copy-start = (bf16[4096,128]{1,0:T(8,128)(2,1)S(1)}, bf16[4096,128]{1,0:T(8,128)(2,1)}, u32[]{:S(2)}) copy-start(bf16[4096,128]{1,0:T(8,128)(2,1)} %param.16) | copy-start | bytes 3145732
  7.2 12.9 %copy-start.2 = (bf16[512,512]{1,0:T(8,128)(2,1)S(1)}, bf16[512,512]{1,0:T(8,128)(2,1)}, u32[]{:S(2)}) copy-start(bf16[512,512]{1,0:T(8,128)(2,1)} %param.12) | copy-start | bytes 1572868
  9.8 25.3 %all-to-all-start.1 = ((bf16[8,512,128]{2,1,0:T(8,128)(2,1)}), bf16[8,512,128]{2,1,0:T(8,128)(2,1)S(1)}, u32[]{:S(2)}, u32[]{:S(2)}) async-start(bf16[8,512,128]{2,1,0:T(8,128)(2,1)} %broadcast_in_dim.10), calls=%async_computation.1 | async-start | bytes 2097152 | tf_op jit(solution)/shard_map/all_to_all | solution.py:22
  36.2 19.4 %all-to-all-start = ((bf16[8,512,128]{2,1,0:T(8,128)(2,1)}), bf16[8,512,128]{2,1,0:T(8,128)(2,1)S(1)}, u32[]{:S(2)}, u32[]{:S(2)}) async-start(bf16[8,512,128]{2,1,0:T(8,128)(2,1)} %broadcast_in_dim.9), calls=%async_computation | async-start | bytes 2097152 | tf_op jit(solution)/shard_map/all_to_all | solution.py:22
  40.6 143.8 %all-reduce.8.cloned.1.call-start = ((), (), s32[]{:S(2)}) async-start(), calls=%async_computation.4 | async-start | bytes 786432
  40.8 15.3 %copy-start.1 = (bf16[512,512]{1,0:T(8,128)(2,1)S(1)}, bf16[512,512]{1,0:T(8,128)(2,1)}, u32[]{:S(2)}) copy-start(bf16[512,512]{1,0:T(8,128)(2,1)} %param.15) | copy-start | bytes 1572868
  40.8 16.3 %copy-start.7 = (bf16[512,256]{1,0:T(8,128)(2,1)S(1)}, bf16[512,256]{1,0:T(8,128)(2,1)}, u32[]{:S(2)}) copy-start(bf16[512,256]{1,0:T(8,128)(2,1)} %param.13) | copy-start | bytes 786436
  55.9 204.3 %copy-start.8 = (f32[128,256]{1,0:T(8,128)S(1)}, f32[128,256]{1,0:T(8,128)}, u32[]{:S(2)}) copy-start(f32[128,256]{1,0:T(8,128)} %param.20) | copy-start | bytes 393220
  55.9 204.3 %copy-start.9 = (f32[128,256]{1,0:T(8,128)S(1)}, f32[128,256]{1,0:T(8,128)}, u32[]{:S(2)}) copy-start(f32[128,256]{1,0:T(8,128)} %param.19) | copy-start | bytes 393220
  56.1 204.8 %copy-start.3 = (f32[128,512]{1,0:T(8,128)S(1)}, f32[128,512]{1,0:T(8,128)}, u32[]{:S(2)}) copy-start(f32[128,512]{1,0:T(8,128)} %param.23) | copy-start | bytes 786436
  56.1 204.8 %copy-start.4 = (f32[128,512]{1,0:T(8,128)S(1)}, f32[128,512]{1,0:T(8,128)}, u32[]{:S(2)}) copy-start(f32[128,512]{1,0:T(8,128)} %param.22) | copy-start | bytes 786436
  58.0 249.8 %copy-start.12 = (f32[64,256]{1,0:T(8,128)S(1)}, f32[64,256]{1,0:T(8,128)}, u32[]{:S(2)}) copy-start(f32[64,256]{1,0:T(8,128)} %param.18) | copy-start | bytes 196612
  260.0 49.6 %copy-start.13 = (f32[32,512]{1,0:T(8,128)S(1)}, f32[32,512]{1,0:T(8,128)}, u32[]{:S(2)}) copy-start(f32[32,512]{1,0:T(8,128)} %param.21) | copy-start | bytes 196612
  260.9 180.3 %copy-start.11 = (f32[128,256]{1,0:T(8,128)}, f32[128,256]{1,0:T(8,128)S(1)}, u32[]{:S(2)}) copy-start(f32[128,256]{1,0:T(8,128)S(1)} %get-tuple-element.20) | copy-start | bytes 393220
  260.9 187.7 %copy-start.10 = (f32[128,256]{1,0:T(8,128)}, f32[128,256]{1,0:T(8,128)S(1)}, u32[]{:S(2)}) copy-start(f32[128,256]{1,0:T(8,128)S(1)} %get-tuple-element.19) | copy-start | bytes 393220
  261.7 179.5 %copy-start.6 = (f32[128,512]{1,0:T(8,128)}, f32[128,512]{1,0:T(8,128)S(1)}, u32[]{:S(2)}) copy-start(f32[128,512]{1,0:T(8,128)S(1)} %get-tuple-element.23) | copy-start | bytes 786436
  261.7 186.9 %copy-start.5 = (f32[128,512]{1,0:T(8,128)}, f32[128,512]{1,0:T(8,128)S(1)}, u32[]{:S(2)}) copy-start(f32[128,512]{1,0:T(8,128)S(1)} %get-tuple-element.22) | copy-start | bytes 786436
  263.6 41.9 %all-to-all-start.2 = ((f32[8,1,2]{2,1,0:T(1,128)}), f32[8,1,2]{2,1,0:T(1,128)S(1)}, u32[]{:S(2)}, u32[]{:S(2)}) async-start(f32[8,1,2]{2,1,0:T(1,128)} %broadcast_in_dim.11), calls=%async_computation.2 | async-start | bytes 8192 | tf_op jit(solution)/shard_map/all_to_all | solution.py:22
  301.0 140.1 %all-gather.5.cloned.1.call-start = ((), (), s32[]{:S(2)}) async-start(), calls=%async_computation.3 | async-start | bytes 4259840 | tf_op jit(solution)/shard_map/all_gather | solution.py:84
  307.8 133.4 %copy-start.14 = (f32[64,256]{1,0:T(8,128)}, f32[64,256]{1,0:T(8,128)S(1)}, u32[]{:S(2)}) copy-start(f32[64,256]{1,0:T(8,128)S(1)} %convolution_multiply_fusion.1) | copy-start | bytes 196612
  309.5 131.6 %copy-start.15 = (f32[32,512]{1,0:T(8,128)}, f32[32,512]{1,0:T(8,128)S(1)}, u32[]{:S(2)}) copy-start(f32[32,512]{1,0:T(8,128)S(1)} %convolution_multiply_fusion) | copy-start | bytes 196612
Sparse Core Ops, SparseCore 0:
  58.1 126.1 all-reduce.7
  311.0 130.1 all-gather.4
where the time goes:
time: 475 us; the launch traced here: 466 us
  waiting for transfers between devices  287 us (60%)
  blocking collectives  72.7 us (15%)
  starting transfers between devices  52.1 us (11%)
  local copies, waits for them, and re-layouts  27.6 us (6%)
  between operations  16.3 us (3%)
  other arithmetic  5.08 us (1%)
  matrix products  4.78 us (1%)
    all_gather x1, waiting for transfers between devices, gather_packed(): lines, at, done = (lax.all_gather(flat, axis), 0, [])  130 us
    unnamed x3, waiting for transfers between devices  123 us
    all_gather x4, blocking collectives, stacked_from(): parts = lax.all_gather(parts, axes[k])  59.4 us
    all_to_all x3, starting transfers between devices, sent_to_all(): return lax.all_to_all(copies, axis, split_axis=0, concat_axis=0, tiled=True)  52.1 us
    all_to_all x3, waiting for transfers between devices, sent_to_all(): return lax.all_to_all(copies, axis, split_axis=0, concat_axis=0, tiled=True)  33.7 us
    unnamed x1, blocking collectives  13.3 us
  transfers between devices with their start and end apart: 5, of which 5 were waited for; matrix products, arithmetic and copies ran while one was open for 1% of the time, Pallas kernels for 0%

commit v1 on v0

v1 whole, which is shorter than its diff:
```python
import jax
import jax.numpy as jnp
from jax import lax
from jax.experimental import pallas as pl
from jax.experimental.pallas import tpu as pltpu
from jax.sharding import Mesh
from jax.sharding import PartitionSpec as P

D = 4096
WIDTH = 2048
R = 128
FS = ("zh", "zl", "y")
Z = ("zh", "zl")
NEAR = ("zl", "y")
FAR = "zh"

BETA_ONE = 0.8
BETA_TWO = 0.9
EPSILON = 1e-08
STEP_RATE = 0.005
FLOOR = 0.25


def sent_to_all(shard, axis):
    copies = jnp.broadcast_to(shard, (lax.axis_size(axis), *shard.shape))
    return lax.all_to_all(copies, axis, split_axis=0, concat_axis=0, tiled=True)


def contract_rows(left, right):
    return lax.dot_general(
        left, right, (((0,), (0,)), ((), ())), preferred_element_type=jnp.float32
    )


def moments(first, second, projected):
    first_new = BETA_ONE * first + (1.0 - BETA_ONE) * projected
    second_new = BETA_TWO * second + (1.0 - BETA_TWO) * projected * projected
    normalized = first_new / (jnp.sqrt(second_new) + EPSILON)
    return (first_new, second_new, normalized)


def split(scaled):
    high = scaled.astype(jnp.bfloat16)
    return high, (scaled - high.astype(jnp.float32)).astype(jnp.bfloat16)


def product(rows, high_ref, low_ref):
    return jnp.dot(rows, high_ref[...], preferred_element_type=jnp.float32) + jnp.dot(
        rows, low_ref[...], preferred_element_type=jnp.float32
    )


def update_kernel(
    scales_ref,
    masters_ref,
    value_factor_ref,
    output_factor_ref,
    value_norm_ref,
    output_norm_ref,
    value_here_ref,
    output_here_ref,
    value_master_ref,
    output_master_ref,
    value_step_ref,
    value_new_ref,
    value_copy_ref,
    output_step_ref,
    output_new_ref,
    output_copy_ref,
    value_high,
    value_low,
    output_high,
    output_low,
):
    @pl.when(pl.program_id(0) == 0)
    def _():
        value_high[...], value_low[...] = split(scales_ref[0] * value_norm_ref[...])
        output_high[...], output_low[...] = split(scales_ref[1] * output_norm_ref[...])
        step = product(value_here_ref[...], value_high, value_low)
        value_step_ref[...] = step
        value_new_ref[...] = value_master_ref[...] - STEP_RATE * step
        step = product(output_here_ref[...], output_high, output_low)
        output_step_ref[...] = step
        output_new_ref[...] = output_master_ref[...] - STEP_RATE * step

    group, packed_rows, width = masters_ref.shape
    value_rows = value_here_ref.shape[0]
    output_rows = output_here_ref.shape[0]
    step = product(value_factor_ref[...], value_high, value_low)
    old = masters_ref[:, :value_rows, :].reshape(group * value_rows, width)
    value_copy_ref[...] = (old.astype(jnp.float32) - STEP_RATE * step).astype(jnp.bfloat16)
    step = product(output_factor_ref[...], output_high, output_low)
    for side in range(2):
        first = value_rows + side * output_rows
        old = masters_ref[:, first : first + output_rows, :].reshape(group * output_rows, width)
        columns = slice(side * width, (side + 1) * width)
        output_copy_ref[:, columns] = (
            old.astype(jnp.float32) - STEP_RATE * step[:, columns]
        ).astype(jnp.bfloat16)


def updated(
    scales,
    masters,
    value_factor,
    output_factor,
    value_norm,
    output_norm,
    value_here,
    output_here,
    value_master,
    output_master,
):
    n_fs, packed_rows, width = masters.shape
    steps = 8
    group = n_fs // steps
    value_rows, value_cols = value_master.shape
    output_rows, output_cols = output_master.shape

    def whole(array):
        return pl.BlockSpec(array.shape, lambda i: (0,) * array.ndim)

    def rows(count, columns):
        return pl.BlockSpec((count, columns), lambda i: (i, 0))

    return pl.pallas_call(
        update_kernel,
        grid=(steps,),
        in_specs=[
            pl.BlockSpec(memory_space=pltpu.SMEM),
            pl.BlockSpec((group, packed_rows, width), lambda i: (i, 0, 0)),
            rows(group * value_rows, R),
            rows(group * output_rows, R),
            whole(value_norm),
            whole(output_norm),
            whole(value_here),
            whole(output_here),
            whole(value_master),
            whole(output_master),
        ],
        out_specs=[
            whole(value_master),
            whole(value_master),
            rows(group * value_rows, value_cols),
            whole(output_master),
            whole(output_master),
            rows(group * output_rows, output_cols),
        ],
        out_shape=[
            jax.ShapeDtypeStruct(value_master.shape, jnp.float32),
            jax.ShapeDtypeStruct(value_master.shape, jnp.float32),
            jax.ShapeDtypeStruct((n_fs * value_rows, value_cols), jnp.bfloat16),
            jax.ShapeDtypeStruct(output_master.shape, jnp.float32),
            jax.ShapeDtypeStruct(output_master.shape, jnp.float32),
            jax.ShapeDtypeStruct((n_fs * output_rows, output_cols), jnp.bfloat16),
        ],
        scratch_shapes=[
            pltpu.VMEM(value_norm.shape, jnp.bfloat16),
            pltpu.VMEM(value_norm.shape, jnp.bfloat16),
            pltpu.VMEM(output_norm.shape, jnp.bfloat16),
            pltpu.VMEM(output_norm.shape, jnp.bfloat16),
        ],
        cost_estimate=pl.CostEstimate(
            flops=4 * R * n_fs * (value_rows * value_cols + output_rows * output_cols),
            bytes_accessed=4 * n_fs * packed_rows * width,
            transcendentals=0,
        ),
        name="update",
    )(
        scales,
        masters,
        value_factor,
        output_factor,
        value_norm,
        output_norm,
        value_here,
        output_here,
        value_master,
        output_master,
    )


def per_device(
    normed_input,
    value_cotangent,
    mixer_output,
    output_cotangent,
    value_factor,
    output_factor,
    value_master,
    value_moment,
    value_second,
    output_master,
    output_moment,
    output_second,
):
    row_index = lax.axis_index(FS)
    column_index = lax.axis_index("tp")
    n_fs = lax.axis_size(FS)
    n_tp = lax.axis_size("tp")
    value_rows, value_cols = value_master.shape
    output_rows, output_cols = output_master.shape
    tokens, feature_cols = normed_input.shape
    head_cols = mixer_output.shape[1]
    half = output_cols // 2

    packed = jnp.concatenate(
        [value_master, output_master[:, :half], output_master[:, half:]], axis=0
    ).astype(jnp.bfloat16)
    plane = sent_to_all(packed, "y")

    factor_features = lax.dynamic_slice_in_dim(
        value_factor, column_index * feature_cols, feature_cols, 0
    )
    factor_heads = lax.dynamic_slice_in_dim(output_factor, column_index * head_cols, head_cols, 0)
    input_partial = jnp.dot(normed_input, factor_features, preferred_element_type=jnp.float32)
    mixer_partial = jnp.dot(mixer_output, factor_heads, preferred_element_type=jnp.float32)
    partial = jnp.concatenate([input_partial, mixer_partial], axis=1).astype(jnp.bfloat16)
    partial = partial.reshape(n_tp, tokens // n_tp, 2 * R)
    partial, plane = lax.optimization_barrier((partial, plane))
    masters = lax.all_gather(plane, Z).reshape(n_fs, *packed.shape)
    blocks = lax.all_to_all(partial, "tp", split_axis=0, concat_axis=0, tiled=True)
    own = jnp.sum(blocks.astype(jnp.float32), axis=0).astype(jnp.bfloat16)
    reduced = sent_to_all(own, "tp").reshape(tokens, 2 * R)

    value_partial = contract_rows(reduced[:, :R], value_cotangent)
    output_partial = contract_rows(reduced[:, R:], output_cotangent)
    n_near = lax.axis_size(NEAR)
    gradient = jnp.concatenate([value_partial, output_partial], axis=1)
    gradient = gradient.reshape(n_near, R // n_near, -1)
    gradient = lax.all_to_all(gradient, NEAR, split_axis=0, concat_axis=0, tiled=True)
    gradient = jnp.sum(gradient, axis=0)
    gradient = jnp.sum(sent_to_all(gradient, FAR), axis=0)
    gradient = sent_to_all(gradient, NEAR).reshape(R, -1)
    value_projected = gradient[:, :value_cols]
    output_projected = gradient[:, value_cols:]

    value_moment_new, value_second_new, value_norm = moments(
        value_moment, value_second, value_projected
    )
    output_moment_new, output_second_new, output_norm = moments(
        output_moment, output_second, output_projected
    )
    totals = jnp.stack([jnp.sum(value_norm * value_norm), jnp.sum(output_norm * output_norm)])
    totals = jnp.sum(sent_to_all(totals.reshape(1, 2), "tp"), axis=(0, 1))
    value_scale = lax.rsqrt(totals[0] / (R * WIDTH) + FLOOR)
    output_scale = lax.rsqrt(totals[1] / (R * D) + FLOOR)

    factor_here = lax.dynamic_slice_in_dim(value_factor, row_index * value_rows, value_rows, 0)
    output_factor_rows = lax.dynamic_slice_in_dim(
        output_factor, row_index * output_rows, output_rows, 0
    )
    scales = jnp.stack([value_scale, output_scale])
    value_step, value_new, value_copy, output_step, output_new, output_copy = updated(
        scales,
        masters,
        value_factor,
        output_factor,
        value_norm,
        output_norm,
        factor_here,
        output_factor_rows,
        value_master,
        output_master,
    )
    return (
        value_step,
        value_new,
        value_copy,
        value_moment_new,
        value_second_new,
        output_step,
        output_new,
        output_copy,
        output_moment_new,
        output_second_new,
    )


def solution(mesh):
    finer = Mesh(mesh.devices.reshape(4, 4, 4, mesh.shape["tp"]), ("zh", "zl", "y", "tp"))
    placed = (
        P(FS, "tp"),
        P(FS, "tp"),
        P(FS, "tp"),
        P(FS, "tp"),
        P(),
        P(),
        P(FS, "tp"),
        P(None, "tp"),
        P(None, "tp"),
        P(FS, "tp"),
        P(None, "tp"),
        P(None, "tp"),
    )
    return jax.shard_map(
        per_device,
        mesh=finer,
        in_specs=placed,
        out_specs=(
            P(FS, "tp"),
            P(FS, "tp"),
            P(None, "tp"),
            P(None, "tp"),
            P(None, "tp"),
            P(FS, "tp"),
            P(FS, "tp"),
            P(None, "tp"),
            P(None, "tp"),
            P(None, "tp"),
        ),
        check_vma=False,
    )
```

time: 475 us -> 149 us (0.31); the launches traced: 466 us -> 148 us
  waiting for transfers between devices: 287 us -> 17.4 us
  starting transfers between devices: 52.1 us -> 16.7 us
  local copies, waits for them, and re-layouts: 27.6 us -> 6.32 us
  Pallas kernels: 0 us -> 8.64 us
    all_gather x1, waiting for transfers between devices: 130 us -> 0.01 us  [per_device(): masters = lax.all_gather(plane, Z).reshape(n_fs, *packed.shape)]
    unnamed x3 -> x1, waiting for transfers between devices: 123 us -> 0.02 us
    all_to_all x0 -> x4, blocking collectives: none -> 73.5 us  [the longest x2 36.1 us: sent_to_all(): return lax.all_to_all(copies, axis, split_axis=0, concat_axis=0, tiled=True)]
    all_gather x4 -> x0, blocking collectives: 59.4 us -> none  [stacked_from(): parts = lax.all_gather(parts, axes[k])]
    all_to_all x3, starting transfers between devices: 52.1 us -> 16.7 us  [sent_to_all(): return lax.all_to_all(copies, axis, split_axis=0, concat_axis=0, tiled=True)]
    all_to_all x3, waiting for transfers between devices: 33.7 us -> 17.4 us  [sent_to_all(): return lax.all_to_all(copies, axis, split_axis=0, concat_axis=0, tiled=True)]
    unnamed x1 -> x0, blocking collectives: 13.3 us -> none
    pallas_call x0 -> x1, Pallas kernels: none -> 8.64 us  [updated(): pl.pallas_call(update_kernel, grid=(steps,), in_specs=[pl.BlockSpec(memor...]
  transfers between devices with their start and end apart: 5 -> 4, of which waited for: 5 -> 3; matrix products, arithmetic and copies ran while one was open for 1% -> 9% of each run, Pallas kernels for 0% -> 0%
where the time goes in v1:
time: 149 us; the launch traced here: 148 us
  blocking collectives  73.5 us (49%)
  waiting for transfers between devices  17.4 us (12%)
  starting transfers between devices  16.7 us (11%)
  between operations  15.6 us (10%)
  Pallas kernels  8.64 us (6%)
  other arithmetic  6.77 us (5%)
  local copies, waits for them, and re-layouts  6.32 us (4%)
  matrix products  2.84 us (2%)
    all_to_all x2, blocking collectives, sent_to_all(): return lax.all_to_all(copies, axis, split_axis=0, concat_axis=0, tiled=True)  36.1 us
    all_to_all x1, blocking collectives, per_device(): lax.all_to_all(gradient, NEAR, split_axis=0, concat_axis=0, tiled=True)  22.1 us
    all_to_all x3, waiting for transfers between devices, sent_to_all(): return lax.all_to_all(copies, axis, split_axis=0, concat_axis=0, tiled=True)  17.4 us
    all_to_all x3, starting transfers between devices, sent_to_all(): return lax.all_to_all(copies, axis, split_axis=0, concat_axis=0, tiled=True)  16.7 us
    all_to_all x1, blocking collectives, per_device(): lax.all_to_all(partial, 'tp', split_axis=0, concat_axis=0, tiled=True)  15.2 us
    pallas_call x1, Pallas kernels, updated(): pl.pallas_call(update_kernel, grid=(steps,), in_specs=[pl.BlockSpec(memor...  8.64 us
  transfers between devices with their start and end apart: 4, of which 3 were waited for; matrix products, arithmetic and copies ran while one was open for 9% of the time, Pallas kernels for 0%

profile of v1, /device:TPU:1, one launch (start us, length us, event | category | flops | bytes accessed | tf_op | source)
XLA Modules:
  0.0 147.7 jit_solution(3447813636058986249)
XLA Ops:
  7.2 0.0 copy-start
  7.2 0.9 convert.22
  8.1 0.8 convert.23
  9.0 0.7 broadcast_in_dim.15
  9.7 5.0 %all-to-all-start = ((bf16[4,128,256]{2,1,0:T(8,128)(2,1)}), bf16[4,128,256]{2,1,0:T(8,128)(2,1)S(1)}, u32[]{:S(2)}, u32[]{:S(2)}) async-start(bf16[4,128,256]{2,1,0:T(8,128)(2,1)} %broadcast_in_dim.15), calls=%async_computation | async-start | bytes 524288 | tf_op jit(solution)/shard_map/all_to_all | solution.py:26
  14.7 1.3 fusion
  16.0 1.1 fusion.1
  17.1 0.1 copy.28
  17.3 0.1 copy.29
  17.4 2.8 %all-to-all-done = bf16[4,128,256]{2,1,0:T(8,128)(2,1)S(1)} async-done(((bf16[4,128,256]{2,1,0:T(8,128)(2,1)}), bf16[4,128,256]{2,1,0:T(8,128)(2,1)S(1)}, u32[]{:S(2)}, u32[]{:S(2)}) %all-to-all-start) | async-done | bytes 262176 | tf_op jit(solution)/shard_map/all_to_all | solution.py:26
  20.2 0.7 copy-done.1
  20.9 0.0 all-gather.3.cloned.1.call-update
  21.0 15.2 %all_to_all.35 = bf16[8,64,256]{2,1,0:T(8,128)(2,1)S(1)} all-to-all(bf16[8,64,256]{2,1,0:T(8,128)(2,1)S(1)} %pad_maximum_fusion), channel_id=1, replica_groups=mesh['zh'=4,'zl'=4,'y'=4,'tp'=8] {'tp'}, dimensions={0} | all-to-all | bytes 524288 | tf_op jit(solution)/shard_map/all_to_all | solution.py:222
  36.3 9.9 %all_to_all.36 = bf16[8,64,256]{2,1,0:T(8,128)(2,1)S(1)} all-to-all(bf16[8,64,256]{2,1,0:T(8,128)(2,1)S(1)} %broadcast_in_dim.16), channel_id=1, replica_groups=mesh['zh'=4,'zl'=4,'y'=4,'tp'=8] {'tp'}, dimensions={0} | all-to-all | bytes 524288 | tf_op jit(solution)/shard_map/all_to_all | solution.py:26
  46.2 0.2 fusion.6
  46.5 0.2 fusion.4
  46.8 22.1 %all_to_all.37 = f32[16,8,768]{2,1,0:T(8,128)S(1)} all-to-all(f32[16,8,768]{2,1,0:T(8,128)S(1)} %maximum_bitcast_fusion), channel_id=1, replica_groups=mesh['zh'=4,'zl'=4,'y'=4,'tp'=8] {'zl','y'}, dimensions={0} | all-to-all | bytes 786432 | tf_op jit(solution)/shard_map/all_to_all | solution.py:231
  68.9 26.2 %all_to_all.38 = f32[4,8,768]{2,1,0:T(8,128)S(1)} all-to-all(f32[4,8,768]{2,1,0:T(8,128)S(1)} %broadcast_in_dim.17), channel_id=1, replica_groups=mesh['zh'=4,'zl'=4,'y'=4,'tp'=8] {'zh'}, dimensions={0} | all-to-all | bytes 196608 | tf_op jit(solution)/shard_map/all_to_all | solution.py:26
  95.1 0.8 broadcast_in_dim.18
  95.9 3.6 %all-to-all-start.5 = ((f32[16,8,768]{2,1,0:T(8,128)}), f32[16,8,768]{2,1,0:T(8,128)S(1)}, u32[]{:S(2)}, u32[]{:S(2)}) async-start(f32[16,8,768]{2,1,0:T(8,128)} %broadcast_in_dim.18), calls=%async_computation.5 | async-start | bytes 786432 | tf_op jit(solution)/shard_map/all_to_all | solution.py:26
  99.5 1.3 constant_dynamic-slice_fusion.1.value_here_ref
  100.8 11.3 %all-to-all-done.5 = f32[16,8,768]{2,1,0:T(8,128)S(1)} async-done(((f32[16,8,768]{2,1,0:T(8,128)}), f32[16,8,768]{2,1,0:T(8,128)S(1)}, u32[]{:S(2)}, u32[]{:S(2)}) %all-to-all-start.5) | async-done | bytes 393248 | tf_op jit(solution)/shard_map/all_to_all | solution.py:26
  112.1 1.4 multiply_reduce_fusion.1
  113.5 1.5 %multiply_reduce_fusion = (f32[]{:T(128)}, f32[128,512]{1,0:T(8,128)}, f32[128,512]{1,0:T(8,128)}, f32[128,512]{1,0:T(8,128)}) fusion(f32[128,768]{1,0:T(8,128)S(1)} %bitcast.17, f32[128,512]{1,0:T(8,128)S(1)} %copy-done.5, f32[128,512]{1,0:T(8,128)S(1)} %copy-done.6), kind=kLoop, calls=%fused_computation.8 | loop fusion | flops 720895 | bytes 1572868 | tf_op jit(solution)/shard_map/reduce_sum | solution.py:244
  115.0 1.4 pad_maximum_fusion.2
  116.4 0.6 broadcast_in_dim.19
  117.0 8.2 %all-to-all-start.6 = ((f32[8,1,2]{2,1,0:T(1,128)}), f32[8,1,2]{2,1,0:T(1,128)S(1)}, u32[]{:S(2)}, u32[]{:S(2)}) async-start(f32[8,1,2]{2,1,0:T(1,128)} %broadcast_in_dim.19), calls=%async_computation.6 | async-start | bytes 8192 | tf_op jit(solution)/shard_map/all_to_all | solution.py:26
  125.2 1.3 constant_dynamic-slice_fusion.output_here_ref
  126.5 3.2 %all-to-all-done.6 = f32[8,1,2]{2,1,0:T(1,128)S(1)} async-done(((f32[8,1,2]{2,1,0:T(1,128)}), f32[8,1,2]{2,1,0:T(1,128)S(1)}, u32[]{:S(2)}, u32[]{:S(2)}) %all-to-all-start.6) | async-done | bytes 96 | tf_op jit(solution)/shard_map/all_to_all | solution.py:26
  129.7 0.6 fusion.15
  131.7 0.6 pad_maximum_fusion.3.scales_ref
  132.3 8.6 %update.1 = (f32[64,256]{1,0:T(8,128)}, f32[64,256]{1,0:T(8,128)}, bf16[4096,256]{1,0:T(8,128)(2,1)}, f32[32,512]{1,0:T(8,128)}, f32[32,512]{1,0:T(8,128)}, /*index=5*/bf16[2048,512]{1,0:T(8,128)(2,1)}) custom-call(f32[2]{0:T(128)} %pad_maximum_fusion.3.scales_ref, bf16[64,128,256]{2,1,0:T(8,128)(2,1)} %all-gather.3.cloned.1.call-done.masters_ref, ...), custom_call_target="tpu_custom_call" | custom-call | flops 1073741824 | bytes 8388608 | tf_op jit(solution)/shard_map/update/pallas_call | solution.py:126
  (28 shorter events, 0.3 us)
Async XLA Ops:
  7.2 7.5 %copy-start = (bf16[512,512]{1,0:T(8,128)(2,1)S(1)}, bf16[512,512]{1,0:T(8,128)(2,1)}, u32[]{:S(2)}) copy-start(bf16[512,512]{1,0:T(8,128)(2,1)} %param.12) | copy-start | bytes 1572868
  7.2 8.8 %copy-start.3 = (bf16[512,256]{1,0:T(8,128)(2,1)S(1)}, bf16[512,256]{1,0:T(8,128)(2,1)}, u32[]{:S(2)}) copy-start(bf16[512,256]{1,0:T(8,128)(2,1)} %param.14) | copy-start | bytes 786436
  9.7 10.5 %all-to-all-start = ((bf16[4,128,256]{2,1,0:T(8,128)(2,1)}), bf16[4,128,256]{2,1,0:T(8,128)(2,1)S(1)}, u32[]{:S(2)}, u32[]{:S(2)}) async-start(bf16[4,128,256]{2,1,0:T(8,128)(2,1)} %broadcast_in_dim.15), calls=%async_computation | async-start | bytes 524288 | tf_op jit(solution)/shard_map/all_to_all | solution.py:26
  14.7 117.5 %all-gather.3.cloned.1.call-start = ((), (), s32[]{:S(2)}) async-start(), calls=%async_computation.7 | async-start | bytes 4456448 | tf_op jit(solution)/shard_map/all_gather | solution.py:221
  14.7 31.5 %copy-start.4 = (bf16[512,256]{1,0:T(8,128)(2,1)S(1)}, bf16[512,256]{1,0:T(8,128)(2,1)}, u32[]{:S(2)}) copy-start(bf16[512,256]{1,0:T(8,128)(2,1)} %param.13) | copy-start | bytes 786436
  16.0 30.4 %copy-start.2 = (bf16[512,512]{1,0:T(8,128)(2,1)S(1)}, bf16[512,512]{1,0:T(8,128)(2,1)}, u32[]{:S(2)}) copy-start(bf16[512,512]{1,0:T(8,128)(2,1)} %param.15) | copy-start | bytes 1572868
  20.2 0.7 copy-start.1
  46.4 65.7 %copy-start.7 = (f32[128,256]{1,0:T(8,128)S(1)}, f32[128,256]{1,0:T(8,128)}, u32[]{:S(2)}) copy-start(f32[128,256]{1,0:T(8,128)} %param.20) | copy-start | bytes 393220
  46.4 65.7 %copy-start.8 = (f32[128,256]{1,0:T(8,128)S(1)}, f32[128,256]{1,0:T(8,128)}, u32[]{:S(2)}) copy-start(f32[128,256]{1,0:T(8,128)} %param.19) | copy-start | bytes 393220
  46.7 66.8 %copy-start.5 = (f32[128,512]{1,0:T(8,128)S(1)}, f32[128,512]{1,0:T(8,128)}, u32[]{:S(2)}) copy-start(f32[128,512]{1,0:T(8,128)} %param.23) | copy-start | bytes 786436
  46.7 66.8 %copy-start.6 = (f32[128,512]{1,0:T(8,128)S(1)}, f32[128,512]{1,0:T(8,128)}, u32[]{:S(2)}) copy-start(f32[128,512]{1,0:T(8,128)} %param.22) | copy-start | bytes 786436
  95.9 16.2 %all-to-all-start.5 = ((f32[16,8,768]{2,1,0:T(8,128)}), f32[16,8,768]{2,1,0:T(8,128)S(1)}, u32[]{:S(2)}, u32[]{:S(2)}) async-start(f32[16,8,768]{2,1,0:T(8,128)} %broadcast_in_dim.18), calls=%async_computation.5 | async-start | bytes 786432 | tf_op jit(solution)/shard_map/all_to_all | solution.py:26
  117.0 12.7 %all-to-all-start.6 = ((f32[8,1,2]{2,1,0:T(1,128)}), f32[8,1,2]{2,1,0:T(1,128)S(1)}, u32[]{:S(2)}, u32[]{:S(2)}) async-start(f32[8,1,2]{2,1,0:T(1,128)} %broadcast_in_dim.19), calls=%async_computation.6 | async-start | bytes 8192 | tf_op jit(solution)/shard_map/all_to_all | solution.py:26
Sparse Core Ops, SparseCore 0:
  21.1 86.6 all-gather.2

commit v2 on v1

v2 whole, which is shorter than its diff:
```python
import jax
import jax.numpy as jnp
from jax import lax
from jax.experimental import pallas as pl
from jax.experimental.pallas import tpu as pltpu
from jax.sharding import Mesh
from jax.sharding import PartitionSpec as P

D = 4096
WIDTH = 2048
R = 128
FS = ("zh", "zl", "y")
Z = ("zh", "zl")
NEAR = ("zl", "y")
FAR = "zh"

BETA_ONE = 0.8
BETA_TWO = 0.9
EPSILON = 1e-08
STEP_RATE = 0.005
FLOOR = 0.25


def sent_to_all(shard, axis):
    copies = jnp.broadcast_to(shard, (lax.axis_size(axis), *shard.shape))
    return lax.all_to_all(copies, axis, split_axis=0, concat_axis=0, tiled=True)


def summed_far(part, axis):
    size = lax.axis_size(axis)

    def shifted(by):
        return lax.ppermute(part, axis, [(i, (i + by) % size) for i in range(size)])

    opposite, before, after = shifted(2), shifted(1), shifted(3)
    return (part + opposite) + (before + after)


def contract_rows(left, right):
    return lax.dot_general(
        left, right, (((0,), (0,)), ((), ())), preferred_element_type=jnp.float32
    )


def moments(first, second, projected):
    first_new = BETA_ONE * first + (1.0 - BETA_ONE) * projected
    second_new = BETA_TWO * second + (1.0 - BETA_TWO) * projected * projected
    normalized = first_new / (jnp.sqrt(second_new) + EPSILON)
    return (first_new, second_new, normalized)


def pack_kernel(value_ref, output_ref, packed_ref):
    copies, packed_rows, width = packed_ref.shape
    value_rows = value_ref.shape[0]
    output_rows = output_ref.shape[0]
    value = value_ref[...].astype(packed_ref.dtype)
    left = output_ref[:, :width].astype(packed_ref.dtype)
    right = output_ref[:, width:].astype(packed_ref.dtype)
    for k in range(copies):
        packed_ref[k, :value_rows, :] = value
        packed_ref[k, value_rows : value_rows + output_rows, :] = left
        packed_ref[k, value_rows + output_rows :, :] = right


def packed_copies(value_master, output_master, copies):
    value_rows, width = value_master.shape
    rows = value_rows + 2 * output_master.shape[0]
    return pl.pallas_call(
        pack_kernel,
        out_shape=jax.ShapeDtypeStruct((copies, rows, width), jnp.bfloat16),
        name="pack",
    )(value_master, output_master)


def project_kernel(index_ref, input_ref, mixer_ref, features_ref, heads_ref, partial_ref):
    blocks, tokens, width = partial_ref.shape
    partial = jnp.dot(input_ref[...], features_ref[...], preferred_element_type=jnp.float32)
    partial_ref[:, :, :R] = partial.astype(jnp.bfloat16).reshape(blocks, tokens, R)
    partial = jnp.dot(mixer_ref[...], heads_ref[...], preferred_element_type=jnp.float32)
    partial_ref[:, :, R:] = partial.astype(jnp.bfloat16).reshape(blocks, tokens, R)


def projected_tokens(index, normed_input, mixer_output, value_factor, output_factor, blocks):
    tokens, features = normed_input.shape
    heads = mixer_output.shape[1]
    return pl.pallas_call(
        project_kernel,
        grid_spec=pltpu.PrefetchScalarGridSpec(
            num_scalar_prefetch=1,
            grid=(1,),
            in_specs=[
                pl.BlockSpec((tokens, features), lambda i, index: (0, 0)),
                pl.BlockSpec((tokens, heads), lambda i, index: (0, 0)),
                pl.BlockSpec((features, R), lambda i, index: (index[0], 0)),
                pl.BlockSpec((heads, R), lambda i, index: (index[0], 0)),
            ],
            out_specs=pl.BlockSpec((blocks, tokens // blocks, 2 * R), lambda i, index: (0, 0, 0)),
        ),
        out_shape=jax.ShapeDtypeStruct((blocks, tokens // blocks, 2 * R), jnp.bfloat16),
        cost_estimate=pl.CostEstimate(
            flops=2 * tokens * (features + heads) * R,
            bytes_accessed=2 * tokens * (features + heads + 2 * R),
            transcendentals=0,
        ),
        name="project",
    )(index, normed_input, mixer_output, value_factor, output_factor)


def norms_kernel(
    gradient_ref,
    value_moment_ref,
    value_second_ref,
    output_moment_ref,
    output_second_ref,
    norm_ref,
    totals_ref,
):
    value_cols = value_moment_ref.shape[1]
    gradient = gradient_ref[...].reshape(R, gradient_ref.shape[2])
    value_norm = moments(value_moment_ref[...], value_second_ref[...], gradient[:, :value_cols])[2]
    output_norm = moments(
        output_moment_ref[...], output_second_ref[...], gradient[:, value_cols:]
    )[2]
    norm_ref[:, :value_cols] = value_norm
    norm_ref[:, value_cols:] = output_norm
    copies, _, lanes = totals_ref.shape
    total = []
    for norm in (value_norm, output_norm):
        squares = jnp.sum(norm * norm, axis=0, keepdims=True)
        total.append(sum(squares[:, k : k + lanes] for k in range(0, norm.shape[1], lanes)))
    for k in range(copies):
        totals_ref[k] = jnp.zeros(totals_ref.shape[1:], jnp.float32)
        totals_ref[k, 0:1, :] = total[0]
        totals_ref[k, 1:2, :] = total[1]


def normed(gradient, value_moment, value_second, output_moment, output_second, copies):
    return pl.pallas_call(
        norms_kernel,
        out_shape=[
            jax.ShapeDtypeStruct((R, gradient.shape[2]), jnp.float32),
            jax.ShapeDtypeStruct((copies, 8, 128), jnp.float32),
        ],
        compiler_params=pltpu.CompilerParams(vmem_limit_bytes=8 << 20),
        name="norms",
    )(gradient, value_moment, value_second, output_moment, output_second)


def inverse_root(totals, row, count):
    total = jnp.sum(totals[row : row + 1, :], axis=1, keepdims=True)
    return lax.rsqrt(total / count + FLOOR)


def product(rows, pair_ref):
    return jnp.dot(
        jnp.concatenate([rows, rows], axis=1), pair_ref[...], preferred_element_type=jnp.float32
    )


def update_kernel(
    row_ref,
    totals_ref,
    norm_ref,
    value_factor_ref,
    output_factor_ref,
    value_master_ref,
    output_master_ref,
    masters_hbm,
    value_step_hbm,
    value_new_hbm,
    value_copy_hbm,
    output_step_hbm,
    output_new_hbm,
    output_copy_hbm,
    masters,
    value_copy,
    output_copy,
    value_step,
    value_new,
    output_step,
    output_new,
    value_pair,
    output_pair,
    in_sems,
    value_sems,
    output_sems,
    own_sems,
):
    chunks = in_sems.shape[0]
    n_fs, _, width = masters.shape
    group = n_fs // chunks
    value_rows, value_cols = value_master_ref.shape
    output_rows = output_master_ref.shape[0]

    def block(k):
        return pl.ds(k * group, group)

    def arriving(k):
        return pltpu.make_async_copy(
            masters_hbm.at[block(k)], masters.at[block(k)], in_sems.at[k]
        )

    def leaving_value(k):
        rows = pl.ds(k * group * value_rows, group * value_rows)
        return pltpu.make_async_copy(value_copy.at[rows], value_copy_hbm.at[rows], value_sems.at[k])

    def leaving_output(k):
        rows = pl.ds(k * group * output_rows, group * output_rows)
        return pltpu.make_async_copy(
            output_copy.at[rows], output_copy_hbm.at[rows], output_sems.at[k]
        )

    for k in range(chunks):
        arriving(k).start()

    totals = jnp.sum(totals_ref[...], axis=0)
    value_scale = inverse_root(totals, 0, R * WIDTH)
    output_scale = inverse_root(totals, 1, R * D)
    for pair, norm, scale in (
        (value_pair, norm_ref[:, :value_cols], value_scale),
        (output_pair, norm_ref[:, value_cols:], output_scale),
    ):
        scaled = (-STEP_RATE * scale) * norm
        high = scaled.astype(jnp.bfloat16)
        pair[:R, :] = high
        pair[R:, :] = (scaled - high.astype(jnp.float32)).astype(jnp.bfloat16)

    row = row_ref[0]
    value_here = value_factor_ref[pl.ds(pl.multiple_of(row * value_rows, value_rows), value_rows), :]
    change = product(value_here, value_pair)
    value_step[...] = change * (-1.0 / STEP_RATE)
    value_new[...] = value_master_ref[...] + change
    output_here = output_factor_ref[
        pl.ds(pl.multiple_of(row * output_rows, output_rows), output_rows), :
    ]
    change = product(output_here, output_pair)
    output_step[...] = change * (-1.0 / STEP_RATE)
    output_new[...] = output_master_ref[...] + change
    own = [
        pltpu.make_async_copy(value_step, value_step_hbm, own_sems.at[0]),
        pltpu.make_async_copy(value_new, value_new_hbm, own_sems.at[1]),
        pltpu.make_async_copy(output_step, output_step_hbm, own_sems.at[2]),
        pltpu.make_async_copy(output_new, output_new_hbm, own_sems.at[3]),
    ]
    for copy in own:
        copy.start()

    for k in range(chunks):
        arriving(k).wait()
        count = group * value_rows
        rows = slice(k * count, (k + 1) * count)
        mine = slice(k * group, (k + 1) * group)
        change = product(value_factor_ref[rows, :], value_pair)
        old = masters[mine, :value_rows, :].reshape(count, width)
        value_copy[rows, :] = (old.astype(jnp.float32) + change).astype(jnp.bfloat16)
        leaving_value(k).start()
        count = group * output_rows
        rows = slice(k * count, (k + 1) * count)
        change = product(output_factor_ref[rows, :], output_pair)
        for side in range(2):
            first = value_rows + side * output_rows
            old = masters[mine, first : first + output_rows, :].reshape(count, width)
            columns = slice(side * width, (side + 1) * width)
            output_copy[rows, columns] = (old.astype(jnp.float32) + change[:, columns]).astype(
                jnp.bfloat16
            )
        leaving_output(k).start()

    for copy in own:
        copy.wait()
    for k in range(chunks):
        leaving_value(k).wait()
        leaving_output(k).wait()


def updated(
    row_index, totals, masters, value_factor, output_factor, norm, value_master, output_master
):
    n_fs, packed_rows, width = masters.shape
    chunks = 4
    value_rows, value_cols = value_master.shape
    output_rows, output_cols = output_master.shape
    in_vmem = pl.BlockSpec(memory_space=pltpu.VMEM)
    anywhere = pl.BlockSpec(memory_space=pl.ANY)
    outs = [
        jax.ShapeDtypeStruct(value_master.shape, jnp.float32),
        jax.ShapeDtypeStruct(value_master.shape, jnp.float32),
        jax.ShapeDtypeStruct((n_fs * value_rows, value_cols), jnp.bfloat16),
        jax.ShapeDtypeStruct(output_master.shape, jnp.float32),
        jax.ShapeDtypeStruct(output_master.shape, jnp.float32),
        jax.ShapeDtypeStruct((n_fs * output_rows, output_cols), jnp.bfloat16),
    ]
    return pl.pallas_call(
        update_kernel,
        in_specs=[pl.BlockSpec(memory_space=pltpu.SMEM)] + [in_vmem] * 6 + [anywhere],
        out_specs=[anywhere] * 6,
        out_shape=outs,
        scratch_shapes=[
            pltpu.VMEM(masters.shape, jnp.bfloat16),
            pltpu.VMEM(outs[2].shape, jnp.bfloat16),
            pltpu.VMEM(outs[5].shape, jnp.bfloat16),
            pltpu.VMEM(value_master.shape, jnp.float32),
            pltpu.VMEM(value_master.shape, jnp.float32),
            pltpu.VMEM(output_master.shape, jnp.float32),
            pltpu.VMEM(output_master.shape, jnp.float32),
            pltpu.VMEM((2 * R, value_cols), jnp.bfloat16),
            pltpu.VMEM((2 * R, output_cols), jnp.bfloat16),
            pltpu.SemaphoreType.DMA((chunks,)),
            pltpu.SemaphoreType.DMA((chunks,)),
            pltpu.SemaphoreType.DMA((chunks,)),
            pltpu.SemaphoreType.DMA((4,)),
        ],
        cost_estimate=pl.CostEstimate(
            flops=4 * R * n_fs * (value_rows * value_cols + output_rows * output_cols),
            bytes_accessed=4 * n_fs * packed_rows * width,
            transcendentals=0,
        ),
        compiler_params=pltpu.CompilerParams(vmem_limit_bytes=57 << 20),
        name="update",
    )(
        row_index,
        totals,
        norm,
        value_factor,
        output_factor,
        value_master,
        output_master,
        masters,
    )


def per_device(
    normed_input,
    value_cotangent,
    mixer_output,
    output_cotangent,
    value_factor,
    output_factor,
    value_master,
    value_moment,
    value_second,
    output_master,
    output_moment,
    output_second,
):
    row_index = lax.axis_index(FS).reshape(1)
    column_index = lax.axis_index("tp").reshape(1)
    n_fs = lax.axis_size(FS)
    n_tp = lax.axis_size("tp")
    tokens = normed_input.shape[0]

    packed = packed_copies(value_master, output_master, lax.axis_size("y"))
    plane = lax.all_to_all(packed, "y", split_axis=0, concat_axis=0, tiled=True)

    partial = projected_tokens(
        column_index, normed_input, mixer_output, value_factor, output_factor, n_tp
    )
    partial, plane = lax.optimization_barrier((partial, plane))
    masters = lax.all_gather(plane, Z).reshape(n_fs, *packed.shape[1:])
    blocks = lax.all_to_all(partial, "tp", split_axis=0, concat_axis=0, tiled=True)
    own = jnp.sum(blocks.astype(jnp.float32), axis=0).astype(jnp.bfloat16)
    reduced = sent_to_all(own, "tp").reshape(tokens, 2 * R)

    value_partial = contract_rows(reduced[:, :R], value_cotangent)
    output_partial = contract_rows(reduced[:, R:], output_cotangent)
    n_y, n_zl = lax.axis_size("y"), lax.axis_size("zl")
    gradient = jnp.concatenate([value_partial, output_partial], axis=1)
    gradient = gradient.reshape(n_y, R // n_y, -1)
    gradient = lax.all_to_all(gradient, "y", split_axis=0, concat_axis=0, tiled=True)
    gradient = jnp.sum(gradient, axis=0).reshape(n_zl, R // n_y // n_zl, -1)
    gradient = lax.all_to_all(gradient, "zl", split_axis=0, concat_axis=0, tiled=True)
    gradient = jnp.sum(gradient, axis=0)
    gradient = summed_far(gradient, FAR)
    gradient = sent_to_all(gradient, ("y", "zl"))

    norm, totals = normed(
        gradient, value_moment, value_second, output_moment, output_second, n_tp
    )
    flat = gradient.reshape(R, -1)
    value_cols = value_master.shape[1]
    value_moment_new, value_second_new, _ = moments(
        value_moment, value_second, flat[:, :value_cols]
    )
    output_moment_new, output_second_new, _ = moments(
        output_moment, output_second, flat[:, value_cols:]
    )
    totals = lax.all_to_all(totals, "tp", split_axis=0, concat_axis=0, tiled=True)
    value_step, value_new, value_copy, output_step, output_new, output_copy = updated(
        row_index, totals, masters, value_factor, output_factor, norm, value_master, output_master
    )
    return (
        value_step,
        value_new,
        value_copy,
        value_moment_new,
        value_second_new,
        output_step,
        output_new,
        output_copy,
        output_moment_new,
        output_second_new,
    )


def solution(mesh):
    finer = Mesh(mesh.devices.reshape(4, 4, 4, mesh.shape["tp"]), ("zh", "zl", "y", "tp"))
    placed = (
        P(FS, "tp"),
        P(FS, "tp"),
        P(FS, "tp"),
        P(FS, "tp"),
        P(),
        P(),
        P(FS, "tp"),
        P(None, "tp"),
        P(None, "tp"),
        P(FS, "tp"),
        P(None, "tp"),
        P(None, "tp"),
    )
    return jax.shard_map(
        per_device,
        mesh=finer,
        in_specs=placed,
        out_specs=(
            P(FS, "tp"),
            P(FS, "tp"),
            P(None, "tp"),
            P(None, "tp"),
            P(None, "tp"),
            P(FS, "tp"),
            P(FS, "tp"),
            P(None, "tp"),
            P(None, "tp"),
            P(None, "tp"),
        ),
        check_vma=False,
    )
```

time: 149 us -> 137 us (0.919)
  blocking collectives: 73.5 us -> 43.7 us
  starting transfers between devices: 16.7 us -> 37.1 us
  waiting for transfers between devices: 17.4 us -> 25.4 us
  other arithmetic: 6.77 us -> 1.73 us
  local copies, waits for them, and re-layouts: 6.32 us -> 2.9 us
  matrix products: 2.84 us -> 0.47 us
  Pallas kernels: 8.64 us -> 10.6 us
    all_to_all x2 -> x1, blocking collectives: 36.1 us -> 9.97 us  [sent_to_all(): return lax.all_to_all(copies, axis, split_axis=0, concat_axis=0, tiled=True)]
    ppermute x0 -> x3, starting transfers between devices: none -> 21.4 us  [shifted(): return lax.ppermute(part, axis, [(i, (i + by) % size) for i in range(size)])]
    all_to_all x3 -> x1, starting transfers between devices: 16.7 us -> 3.55 us  [sent_to_all(): return lax.all_to_all(copies, axis, split_axis=0, concat_axis=0, tiled=True)]
    all_to_all x0 -> x2, starting transfers between devices: none -> 12.2 us  [the longest x1 7.2 us: per_device(): lax.all_to_all(totals, 'tp', split_axis=0, concat_axis=0, tiled=True)]
    all_to_all x0 -> x2, waiting for transfers between devices: none -> 6.38 us  [the longest x1 3.26 us: per_device(): plane = lax.all_to_all(packed, 'y', split_axis=0, concat_axis=0, tiled=True)]
    ppermute x0 -> x3, waiting for transfers between devices: none -> 4.82 us  [shifted(): return lax.ppermute(part, axis, [(i, (i + by) % size) for i in range(size)])]
    all_to_all x1 -> x2, blocking collectives: 22.1 us -> 17.6 us  [the longest x1 9.71 us: per_device(): lax.all_to_all(gradient, 'y', split_axis=0, concat_axis=0, tiled=True)]
    another operation x4 -> x0, other arithmetic: 3.68 us -> none
  transfers between devices with their start and end apart: 4 -> 7, of which waited for: 3 -> 5; matrix products, arithmetic and copies ran while one was open for 9% -> 2% of each run, Pallas kernels for 0% -> 2%
where the time goes in v2:
time: 137 us; the launch traced here: 136 us
  blocking collectives  43.7 us (32%)
  starting transfers between devices  37.1 us (27%)
  waiting for transfers between devices  25.4 us (19%)
  between operations  14.2 us (10%)
  Pallas kernels  10.6 us (8%)
  local copies, waits for them, and re-layouts  2.9 us (2%)
  other arithmetic  1.73 us (1%)
    ppermute x3, starting transfers between devices, shifted(): return lax.ppermute(part, axis, [(i, (i + by) % size) for i in range(size)])  21.4 us
    all_to_all x1, blocking collectives, per_device(): lax.all_to_all(partial, 'tp', split_axis=0, concat_axis=0, tiled=True)  16.2 us
    all_to_all x1, waiting for transfers between devices, sent_to_all(): return lax.all_to_all(copies, axis, split_axis=0, concat_axis=0, tiled=True)  14.2 us
    all_to_all x1, blocking collectives, sent_to_all(): return lax.all_to_all(copies, axis, split_axis=0, concat_axis=0, tiled=True)  9.97 us
    all_to_all x1, blocking collectives, per_device(): lax.all_to_all(gradient, 'y', split_axis=0, concat_axis=0, tiled=True)  9.71 us
    all_to_all x1, blocking collectives, per_device(): lax.all_to_all(gradient, 'zl', split_axis=0, concat_axis=0, tiled=True)  7.88 us
    all_to_all x1, starting transfers between devices, per_device(): lax.all_to_all(totals, 'tp', split_axis=0, concat_axis=0, tiled=True)  7.2 us
    pallas_call x1, Pallas kernels, updated(): pl.pallas_call(update_kernel, in_specs=[pl.BlockSpec(memory_space=pltpu.S...  5.72 us
  transfers between devices with their start and end apart: 7, of which 5 were waited for; matrix products, arithmetic and copies ran while one was open for 2% of the time, Pallas kernels for 2%

profile of v2, /device:TPU:1, one launch (start us, length us, event | category | flops | bytes accessed | tf_op | source)
XLA Modules:
  0.0 136.1 jit_solution(3306683076941190466)
XLA Ops:
  7.2 0.0 copy-start
  7.2 1.7 %pack.1 = bf16[4,128,256]{2,1,0:T(8,128)(2,1)} custom-call(f32[64,256]{1,0:T(8,128)} %value_master_ref.1, f32[32,512]{1,0:T(8,128)} %output_master_ref.1), custom_call_target="tpu_custom_call" | custom-call | tf_op jit(solution)/shard_map/pack/pallas_call | solution.py:68
  8.8 5.0 %all-to-all-start = ((bf16[4,128,256]{2,1,0:T(8,128)(2,1)}), bf16[4,128,256]{2,1,0:T(8,128)(2,1)S(1)}, u32[]{:S(2)}, u32[]{:S(2)}) async-start(bf16[4,128,256]{2,1,0:T(8,128)(2,1)} %pack.1), calls=%async_computation | async-start | bytes 524288 | tf_op jit(solution)/shard_map/all_to_all | solution.py:353
  13.8 2.3 %project.1 = bf16[8,64,256]{2,1,0:T(8,128)(2,1)} custom-call(s32[1]{0:T(128)} %bitcast.1.index_ref, bf16[512,512]{1,0:T(8,128)(2,1)} %input_ref.1, bf16[512,256]{1,0:T(8,128)(2,1)} %mixer_ref.1, bf16[4096,128]{1,0:T(8,128)(2,1)} %value_factor_ref.1, bf16[2048,128]{1,0:T(8,128)(2,1)} %output_factor_ref.1), custom_call_target="tpu_custom_call" | custom-call | flops 100663296 | bytes 1048576 | tf_op jit(solution)/shard_map/project/pallas_call | solution.py:86
  16.1 3.3 %all-to-all-done = bf16[4,128,256]{2,1,0:T(8,128)(2,1)S(1)} async-done(((bf16[4,128,256]{2,1,0:T(8,128)(2,1)}), bf16[4,128,256]{2,1,0:T(8,128)(2,1)S(1)}, u32[]{:S(2)}, u32[]{:S(2)}) %all-to-all-start) | async-done | bytes 262176 | tf_op jit(solution)/shard_map/all_to_all | solution.py:353
  19.4 0.7 copy-done.6
  20.1 0.0 all-gather.3.cloned.1.call-update
  20.1 16.2 %all_to_all.35 = bf16[8,64,256]{2,1,0:T(8,128)(2,1)S(1)} all-to-all(bf16[8,64,256]{2,1,0:T(8,128)(2,1)} %project.1), channel_id=1, replica_groups=mesh['zh'=4,'zl'=4,'y'=4,'tp'=8] {'tp'}, dimensions={0} | all-to-all | bytes 524288 | tf_op jit(solution)/shard_map/all_to_all | solution.py:360
  36.3 10.0 %all_to_all.36 = bf16[8,64,256]{2,1,0:T(8,128)(2,1)S(1)} all-to-all(bf16[8,64,256]{2,1,0:T(8,128)(2,1)S(1)} %broadcast_in_dim.6), channel_id=1, replica_groups=mesh['zh'=4,'zl'=4,'y'=4,'tp'=8] {'tp'}, dimensions={0} | all-to-all | bytes 524288 | tf_op jit(solution)/shard_map/all_to_all | solution.py:26
  46.3 0.2 fusion.4
  46.5 0.2 fusion.2
  46.8 0.0 copy-start.1
  46.8 0.0 copy-start.2
  46.8 0.0 copy-start.3
  46.9 9.7 %all_to_all.37 = f32[4,32,768]{2,1,0:T(8,128)S(1)} all-to-all(f32[4,32,768]{2,1,0:T(8,128)S(1)} %bitcast.10), channel_id=1, replica_groups=mesh['zh'=4,'zl'=4,'y'=4,'tp'=8] {'y'}, dimensions={0} | all-to-all | bytes 786432 | tf_op jit(solution)/shard_map/all_to_all | solution.py:369
  56.6 7.9 %all_to_all.38 = f32[4,8,768]{2,1,0:T(8,128)S(1)} all-to-all(f32[4,8,768]{2,1,0:T(8,128)S(1)} %bitcast.13), channel_id=1, replica_groups=mesh['zh'=4,'zl'=4,'y'=4,'tp'=8] {'zl'}, dimensions={0} | all-to-all | bytes 196608 | tf_op jit(solution)/shard_map/all_to_all | solution.py:371
  64.5 12.2 %collective-permute-start = (f32[8,768]{1,0:T(8,128)S(1)}, f32[8,768]{1,0:T(8,128)S(1)}, u32[]{:S(2)}, u32[]{:S(2)}) collective-permute-start(f32[8,768]{1,0:T(8,128)S(1)} %reduce_sum.32), channel_id=1, source_target_pairs={{0,256},{128,384},{256,0},{384,128},{1,257},{129,385},{257,1},{385... | collective-permute-start | bytes 73736 | tf_op jit(solution)/shard_map/ppermute | solution.py:33
  76.7 4.8 %collective-permute-start.1 = (f32[8,768]{1,0:T(8,128)S(1)}, f32[8,768]{1,0:T(8,128)S(1)}, u32[]{:S(2)}, u32[]{:S(2)}) collective-permute-start(f32[8,768]{1,0:T(8,128)S(1)} %reduce_sum.32), channel_id=1, source_target_pairs={{0,128},{128,256},{256,384},{384,0},{1,129},{129,257},{257,385},{3... | collective-permute-start | bytes 73736 | tf_op jit(solution)/shard_map/ppermute | solution.py:33
  81.5 4.4 %collective-permute-start.2 = (f32[8,768]{1,0:T(8,128)S(1)}, f32[8,768]{1,0:T(8,128)S(1)}, u32[]{:S(2)}, u32[]{:S(2)}) collective-permute-start(f32[8,768]{1,0:T(8,128)S(1)} %reduce_sum.32), channel_id=1, source_target_pairs={{0,384},{128,0},{256,128},{384,256},{1,385},{129,1},{257,129},{385... | collective-permute-start | bytes 73736 | tf_op jit(solution)/shard_map/ppermute | solution.py:33
  85.9 0.1 collective-permute-done.1
  86.0 4.7 %collective-permute-done.2 = f32[8,768]{1,0:T(8,128)S(1)} collective-permute-done((f32[8,768]{1,0:T(8,128)S(1)}, f32[8,768]{1,0:T(8,128)S(1)}, u32[]{:S(2)}, u32[]{:S(2)}) %collective-permute-start.2) | collective-permute-done | bytes 24608 | tf_op jit(solution)/shard_map/ppermute | solution.py:33
  90.7 0.8 broadcast_in_dim.7
  91.5 3.6 %all-to-all-start.5 = ((f32[16,8,768]{2,1,0:T(8,128)}), f32[16,8,768]{2,1,0:T(8,128)S(1)}, u32[]{:S(2)}, u32[]{:S(2)}) async-start(f32[16,8,768]{2,1,0:T(8,128)} %broadcast_in_dim.7), calls=%async_computation.5 | async-start | bytes 786432 | tf_op jit(solution)/shard_map/all_to_all | solution.py:26
  95.1 14.2 %all-to-all-done.5.gradient_ref = f32[16,8,768]{2,1,0:T(8,128)S(1)} async-done(((f32[16,8,768]{2,1,0:T(8,128)}), f32[16,8,768]{2,1,0:T(8,128)S(1)}, u32[]{:S(2)}, u32[]{:S(2)}) %all-to-all-start.5) | async-done | bytes 393248 | tf_op jit(solution)/shard_map/all_to_all | solution.py:26
  109.3 0.9 norms.1
  110.2 0.8 copy-done.5
  111.0 7.2 %all-to-all-start.6 = ((f32[8,8,128]{2,1,0:T(8,128)}), f32[8,8,128]{2,1,0:T(8,128)S(1)}, u32[]{:S(2)}, u32[]{:S(2)}) async-start(f32[8,8,128]{2,1,0:T(8,128)} %get-tuple-element.21), calls=%async_computation.6 | async-start | bytes 65536 | tf_op jit(solution)/shard_map/all_to_all | solution.py:387
  118.2 0.9 fusion
  119.1 0.7 fusion.1
  119.8 3.1 %all-to-all-done.6.totals_ref = f32[8,8,128]{2,1,0:T(8,128)S(1)} async-done(((f32[8,8,128]{2,1,0:T(8,128)}), f32[8,8,128]{2,1,0:T(8,128)S(1)}, u32[]{:S(2)}, u32[]{:S(2)}) %all-to-all-start.6) | async-done | bytes 32800 | tf_op jit(solution)/shard_map/all_to_all | solution.py:387
  122.9 0.6 copy-done.8
  123.5 5.7 %update.1 = (f32[64,256]{1,0:T(8,128)}, f32[64,256]{1,0:T(8,128)}, bf16[4096,256]{1,0:T(8,128)(2,1)}, f32[32,512]{1,0:T(8,128)}, f32[32,512]{1,0:T(8,128)}, /*index=5*/bf16[2048,512]{1,0:T(8,128)(2,1)}) custom-call(s32[1]{0:T(128)} %bitcast.row_ref, f32[8,8,128]{2,1,0:T(8,128)} %copy-done.8, f32[128,768]{1,0:T(8,128)} %copy-done.5, ...), custom_call_target="tpu_custom_call" | custom-call | flops 1073741824 | bytes 8388608 | tf_op jit(solution)/shard_map/update/pallas_call | solution.py:293
  (20 shorter events, 0.2 us)
Async XLA Ops:
  7.2 39.4 %copy-start = (bf16[512,512]{1,0:T(8,128)(2,1)S(1)}, bf16[512,512]{1,0:T(8,128)(2,1)}, u32[]{:S(2)}) copy-start(bf16[512,512]{1,0:T(8,128)(2,1)} %param.15) | copy-start | bytes 1572868
  8.8 10.5 %all-to-all-start = ((bf16[4,128,256]{2,1,0:T(8,128)(2,1)}), bf16[4,128,256]{2,1,0:T(8,128)(2,1)S(1)}, u32[]{:S(2)}, u32[]{:S(2)}) async-start(bf16[4,128,256]{2,1,0:T(8,128)(2,1)} %pack.1), calls=%async_computation | async-start | bytes 524288 | tf_op jit(solution)/shard_map/all_to_all | solution.py:353
  13.8 109.1 %all-gather.3.cloned.1.call-start = ((), (), s32[]{:S(2)}) async-start(), calls=%async_computation.7 | async-start | bytes 4456448 | tf_op jit(solution)/shard_map/all_gather | solution.py:359
  13.8 32.5 %copy-start.7 = (bf16[512,256]{1,0:T(8,128)(2,1)S(1)}, bf16[512,256]{1,0:T(8,128)(2,1)}, u32[]{:S(2)}) copy-start(bf16[512,256]{1,0:T(8,128)(2,1)} %param.13) | copy-start | bytes 786436
  19.4 0.7 copy-start.6
  46.8 62.5 %copy-start.1 = (f32[128,512]{1,0:T(8,128)S(1)}, f32[128,512]{1,0:T(8,128)}, u32[]{:S(2)}) copy-start(f32[128,512]{1,0:T(8,128)} %output_moment_ref.1) | copy-start | bytes 786436
  46.8 62.4 %copy-start.2 = (f32[128,512]{1,0:T(8,128)S(1)}, f32[128,512]{1,0:T(8,128)}, u32[]{:S(2)}) copy-start(f32[128,512]{1,0:T(8,128)} %output_second_ref.1) | copy-start | bytes 786436
  46.8 62.4 %copy-start.3 = (f32[128,256]{1,0:T(8,128)S(1)}, f32[128,256]{1,0:T(8,128)}, u32[]{:S(2)}) copy-start(f32[128,256]{1,0:T(8,128)} %value_moment_ref.1) | copy-start | bytes 393220
  46.8 62.4 %copy-start.4 = (f32[128,256]{1,0:T(8,128)S(1)}, f32[128,256]{1,0:T(8,128)}, u32[]{:S(2)}) copy-start(f32[128,256]{1,0:T(8,128)} %value_second_ref.1) | copy-start | bytes 393220
  64.5 21.4 %collective-permute-start = (f32[8,768]{1,0:T(8,128)S(1)}, f32[8,768]{1,0:T(8,128)S(1)}, u32[]{:S(2)}, u32[]{:S(2)}) collective-permute-start(f32[8,768]{1,0:T(8,128)S(1)} %reduce_sum.32), channel_id=1, source_target_pairs={{0,256},{128,384},{256,0},{384,128},{1,257},{129,385},{257,1},{385... | collective-permute-start | bytes 73736 | tf_op jit(solution)/shard_map/ppermute | solution.py:33
  76.7 9.3 %collective-permute-start.1 = (f32[8,768]{1,0:T(8,128)S(1)}, f32[8,768]{1,0:T(8,128)S(1)}, u32[]{:S(2)}, u32[]{:S(2)}) collective-permute-start(f32[8,768]{1,0:T(8,128)S(1)} %reduce_sum.32), channel_id=1, source_target_pairs={{0,128},{128,256},{256,384},{384,0},{1,129},{129,257},{257,385},{3... | collective-permute-start | bytes 73736 | tf_op jit(solution)/shard_map/ppermute | solution.py:33
  81.5 9.2 %collective-permute-start.2 = (f32[8,768]{1,0:T(8,128)S(1)}, f32[8,768]{1,0:T(8,128)S(1)}, u32[]{:S(2)}, u32[]{:S(2)}) collective-permute-start(f32[8,768]{1,0:T(8,128)S(1)} %reduce_sum.32), channel_id=1, source_target_pairs={{0,384},{128,0},{256,128},{384,256},{1,385},{129,1},{257,129},{385... | collective-permute-start | bytes 73736 | tf_op jit(solution)/shard_map/ppermute | solution.py:33
  91.5 17.7 %all-to-all-start.5 = ((f32[16,8,768]{2,1,0:T(8,128)}), f32[16,8,768]{2,1,0:T(8,128)S(1)}, u32[]{:S(2)}, u32[]{:S(2)}) async-start(f32[16,8,768]{2,1,0:T(8,128)} %broadcast_in_dim.7), calls=%async_computation.5 | async-start | bytes 786432 | tf_op jit(solution)/shard_map/all_to_all | solution.py:26
  110.2 0.8 copy-start.5
  111.0 11.9 %all-to-all-start.6 = ((f32[8,8,128]{2,1,0:T(8,128)}), f32[8,8,128]{2,1,0:T(8,128)S(1)}, u32[]{:S(2)}, u32[]{:S(2)}) async-start(f32[8,8,128]{2,1,0:T(8,128)} %get-tuple-element.21), calls=%async_computation.6 | async-start | bytes 65536 | tf_op jit(solution)/shard_map/all_to_all | solution.py:387
  122.9 0.6 copy-start.8
Sparse Core Ops, SparseCore 0:
  20.2 78.2 all-gather.2

commit v3 on v2

--- a/solution.py
+++ b/solution.py
@@ -116,7 +116,7 @@
     totals_ref,
 ):
     value_cols = value_moment_ref.shape[1]
-    gradient = gradient_ref[...].reshape(R, gradient_ref.shape[2])
+    gradient = gradient_ref[...].astype(jnp.float32).reshape(R, gradient_ref.shape[2])
     value_norm = moments(value_moment_ref[...], value_second_ref[...], gradient[:, :value_cols])[2]
     output_norm = moments(
         output_moment_ref[...], output_second_ref[...], gradient[:, value_cols:]
@@ -315,7 +315,7 @@
             bytes_accessed=4 * n_fs * packed_rows * width,
             transcendentals=0,
         ),
-        compiler_params=pltpu.CompilerParams(vmem_limit_bytes=57 << 20),
+        compiler_params=pltpu.CompilerParams(vmem_limit_bytes=52 << 20),
         name="update",
     )(
         row_index,
@@ -355,7 +355,7 @@
     partial = projected_tokens(
         column_index, normed_input, mixer_output, value_factor, output_factor, n_tp
     )
-    partial, plane = lax.optimization_barrier((partial, plane))
+    partial, plane, row_index = lax.optimization_barrier((partial, plane, row_index))
     masters = lax.all_gather(plane, Z).reshape(n_fs, *packed.shape[1:])
     blocks = lax.all_to_all(partial, "tp", split_axis=0, concat_axis=0, tiled=True)
     own = jnp.sum(blocks.astype(jnp.float32), axis=0).astype(jnp.bfloat16)
@@ -371,12 +371,12 @@
     gradient = lax.all_to_all(gradient, "zl", split_axis=0, concat_axis=0, tiled=True)
     gradient = jnp.sum(gradient, axis=0)
     gradient = summed_far(gradient, FAR)
-    gradient = sent_to_all(gradient, ("y", "zl"))
+    gradient = sent_to_all(gradient.astype(jnp.bfloat16), ("y", "zl"))
 
     norm, totals = normed(
         gradient, value_moment, value_second, output_moment, output_second, n_tp
     )
-    flat = gradient.reshape(R, -1)
+    flat = gradient.astype(jnp.float32).reshape(R, -1)
     value_cols = value_master.shape[1]
     value_moment_new, value_second_new, _ = moments(
         value_moment, value_second, flat[:, :value_cols]

time: 137 us -> 130 us (0.949)
  waiting for transfers between devices: 25.4 us -> 10.5 us
  blocking collectives: 43.7 us -> 56 us
  starting transfers between devices: 37.1 us -> 34.9 us
  local copies, waits for them, and re-layouts: 2.9 us -> 0.79 us
    all_to_all x1 -> x0, waiting for transfers between devices: 14.2 us -> none  [sent_to_all(): return lax.all_to_all(copies, axis, split_axis=0, concat_axis=0, tiled=True)]
    all_to_all x1 -> x2, blocking collectives: 9.97 us -> 22.2 us  [sent_to_all(): return lax.all_to_all(copies, axis, split_axis=0, concat_axis=0, tiled=True)]
    all_to_all x1 -> x0, starting transfers between devices: 3.55 us -> none  [sent_to_all(): return lax.all_to_all(copies, axis, split_axis=0, concat_axis=0, tiled=True)]
  transfers between devices with their start and end apart: 7 -> 6, of which waited for: 5 -> 3; matrix products, arithmetic and copies ran while one was open for 2% -> 2% of each run, Pallas kernels for 2% -> 2%
where the time goes in v3:
time: 130 us; the launch traced here: 129 us
  blocking collectives  56 us (43%)
  starting transfers between devices  34.9 us (27%)
  between operations  14.2 us (11%)
  waiting for transfers between devices  10.5 us (8%)
  Pallas kernels  10.4 us (8%)
  other arithmetic  1.76 us (1%)
    all_to_all x2, blocking collectives, sent_to_all(): return lax.all_to_all(copies, axis, split_axis=0, concat_axis=0, tiled=True)  22.2 us
    ppermute x3, starting transfers between devices, shifted(): return lax.ppermute(part, axis, [(i, (i + by) % size) for i in range(size)])  21.5 us
    all_to_all x1, blocking collectives, per_device(): lax.all_to_all(partial, 'tp', split_axis=0, concat_axis=0, tiled=True)  16.2 us
    all_to_all x1, blocking collectives, per_device(): lax.all_to_all(gradient, 'y', split_axis=0, concat_axis=0, tiled=True)  9.58 us
    all_to_all x1, starting transfers between devices, per_device(): lax.all_to_all(totals, 'tp', split_axis=0, concat_axis=0, tiled=True)  8.42 us
    all_to_all x1, blocking collectives, per_device(): lax.all_to_all(gradient, 'zl', split_axis=0, concat_axis=0, tiled=True)  8.11 us
    pallas_call x1, Pallas kernels, updated(): pl.pallas_call(update_kernel, in_specs=[pl.BlockSpec(memory_space=pltpu.S...  5.56 us
    all_to_all x1, starting transfers between devices, per_device(): plane = lax.all_to_all(packed, 'y', split_axis=0, concat_axis=0, tiled=True)  5 us
  transfers between devices with their start and end apart: 6, of which 3 were waited for; matrix products, arithmetic and copies ran while one was open for 2% of the time, Pallas kernels for 2%

profile of v3, /device:TPU:1, one launch (start us, length us, event | category | flops | bytes accessed | tf_op | source)
XLA Modules:
  0.0 129.1 jit_solution(12521932282829988806)
XLA Ops:
  7.2 0.0 copy-start
  7.2 1.7 %pack.1 = bf16[4,128,256]{2,1,0:T(8,128)(2,1)} custom-call(f32[64,256]{1,0:T(8,128)} %value_master_ref.1, f32[32,512]{1,0:T(8,128)} %output_master_ref.1), custom_call_target="tpu_custom_call" | custom-call | tf_op jit(solution)/shard_map/pack/pallas_call | solution.py:68
  8.8 5.0 %all-to-all-start = ((bf16[4,128,256]{2,1,0:T(8,128)(2,1)}), bf16[4,128,256]{2,1,0:T(8,128)(2,1)S(1)}, u32[]{:S(2)}, u32[]{:S(2)}) async-start(bf16[4,128,256]{2,1,0:T(8,128)(2,1)} %pack.1), calls=%async_computation | async-start | bytes 524288 | tf_op jit(solution)/shard_map/all_to_all | solution.py:353
  13.8 2.3 %project.1 = bf16[8,64,256]{2,1,0:T(8,128)(2,1)} custom-call(s32[1]{0:T(128)} %bitcast.index_ref, bf16[512,512]{1,0:T(8,128)(2,1)} %input_ref.1, bf16[512,256]{1,0:T(8,128)(2,1)} %mixer_ref.1, bf16[4096,128]{1,0:T(8,128)(2,1)} %value_factor_ref.1, bf16[2048,128]{1,0:T(8,128)(2,1)} %output_factor_ref.1), custom_call_target="tpu_custom_call" | custom-call | flops 100663296 | bytes 1048576 | tf_op jit(solution)/shard_map/project/pallas_call | solution.py:86
  16.1 3.3 %all-to-all-done = bf16[4,128,256]{2,1,0:T(8,128)(2,1)S(1)} async-done(((bf16[4,128,256]{2,1,0:T(8,128)(2,1)}), bf16[4,128,256]{2,1,0:T(8,128)(2,1)S(1)}, u32[]{:S(2)}, u32[]{:S(2)}) %all-to-all-start) | async-done | bytes 262176 | tf_op jit(solution)/shard_map/all_to_all | solution.py:353
  19.4 0.7 copy-done.8
  20.1 0.0 all-gather.3.cloned.1.call-update
  20.1 16.2 %all_to_all.35 = bf16[8,64,256]{2,1,0:T(8,128)(2,1)S(1)} all-to-all(bf16[8,64,256]{2,1,0:T(8,128)(2,1)} %project.1), channel_id=1, replica_groups=mesh['zh'=4,'zl'=4,'y'=4,'tp'=8] {'tp'}, dimensions={0} | all-to-all | bytes 524288 | tf_op jit(solution)/shard_map/all_to_all | solution.py:360
  36.3 10.0 %all_to_all.36 = bf16[8,64,256]{2,1,0:T(8,128)(2,1)S(1)} all-to-all(bf16[8,64,256]{2,1,0:T(8,128)(2,1)S(1)} %broadcast_in_dim.6), channel_id=1, replica_groups=mesh['zh'=4,'zl'=4,'y'=4,'tp'=8] {'tp'}, dimensions={0} | all-to-all | bytes 524288 | tf_op jit(solution)/shard_map/all_to_all | solution.py:26
  46.3 0.2 fusion.4
  46.5 0.0 copy-start.2
  46.6 0.0 copy-start.3
  46.6 0.0 copy-start.4
  46.6 0.0 copy-start.5
  46.6 0.2 fusion.2
  46.9 9.6 %all_to_all.37 = f32[4,32,768]{2,1,0:T(8,128)S(1)} all-to-all(f32[4,32,768]{2,1,0:T(8,128)S(1)} %bitcast.10), channel_id=1, replica_groups=mesh['zh'=4,'zl'=4,'y'=4,'tp'=8] {'y'}, dimensions={0} | all-to-all | bytes 786432 | tf_op jit(solution)/shard_map/all_to_all | solution.py:369
  56.5 8.1 %all_to_all.38 = f32[4,8,768]{2,1,0:T(8,128)S(1)} all-to-all(f32[4,8,768]{2,1,0:T(8,128)S(1)} %bitcast.13), channel_id=1, replica_groups=mesh['zh'=4,'zl'=4,'y'=4,'tp'=8] {'zl'}, dimensions={0} | all-to-all | bytes 196608 | tf_op jit(solution)/shard_map/all_to_all | solution.py:371
  64.6 12.3 %collective-permute-start = (f32[8,768]{1,0:T(8,128)S(1)}, f32[8,768]{1,0:T(8,128)S(1)}, u32[]{:S(2)}, u32[]{:S(2)}) collective-permute-start(f32[8,768]{1,0:T(8,128)S(1)} %reduce_sum.32), channel_id=1, source_target_pairs={{0,256},{128,384},{256,0},{384,128},{1,257},{129,385},{257,1},{385... | collective-permute-start | bytes 73736 | tf_op jit(solution)/shard_map/ppermute | solution.py:33
  76.9 4.3 %collective-permute-start.1 = (f32[8,768]{1,0:T(8,128)S(1)}, f32[8,768]{1,0:T(8,128)S(1)}, u32[]{:S(2)}, u32[]{:S(2)}) collective-permute-start(f32[8,768]{1,0:T(8,128)S(1)} %reduce_sum.32), channel_id=1, source_target_pairs={{0,128},{128,256},{256,384},{384,0},{1,129},{129,257},{257,385},{3... | collective-permute-start | bytes 73736 | tf_op jit(solution)/shard_map/ppermute | solution.py:33
  81.2 4.9 %collective-permute-start.2 = (f32[8,768]{1,0:T(8,128)S(1)}, f32[8,768]{1,0:T(8,128)S(1)}, u32[]{:S(2)}, u32[]{:S(2)}) collective-permute-start(f32[8,768]{1,0:T(8,128)S(1)} %reduce_sum.32), channel_id=1, source_target_pairs={{0,384},{128,0},{256,128},{384,256},{1,385},{129,1},{257,129},{385... | collective-permute-start | bytes 73736 | tf_op jit(solution)/shard_map/ppermute | solution.py:33
  86.1 0.0 collective-permute-done
  86.1 0.0 collective-permute-done.1
  86.2 4.1 %collective-permute-done.2 = f32[8,768]{1,0:T(8,128)S(1)} collective-permute-done((f32[8,768]{1,0:T(8,128)S(1)}, f32[8,768]{1,0:T(8,128)S(1)}, u32[]{:S(2)}, u32[]{:S(2)}) %collective-permute-start.2) | collective-permute-done | bytes 24608 | tf_op jit(solution)/shard_map/ppermute | solution.py:33
  90.3 0.0 copy-start.6
  90.3 0.0 copy-start.7
  90.3 12.2 %all_to_all.39.gradient_ref = bf16[16,8,768]{2,1,0:T(8,128)(2,1)S(1)} all-to-all(bf16[16,8,768]{2,1,0:T(8,128)(2,1)S(1)} %broadcast_in_dim.7), channel_id=1, replica_groups=mesh['zh'=4,'zl'=4,'y'=4,'tp'=8] {'y','zl'}, dimensions={0} | all-to-all | bytes 393216 | tf_op jit(solution)/shard_map/all_to_all | solution.py:26
  102.6 1.0 norms.1
  103.5 8.4 %all-to-all-start.6 = ((f32[8,8,128]{2,1,0:T(8,128)}), f32[8,8,128]{2,1,0:T(8,128)S(1)}, u32[]{:S(2)}, u32[]{:S(2)}) async-start(f32[8,8,128]{2,1,0:T(8,128)} %get-tuple-element.23), calls=%async_computation.6 | async-start | bytes 65536 | tf_op jit(solution)/shard_map/all_to_all | solution.py:387
  112.0 0.9 fusion
  112.9 0.7 fusion.1
  113.6 3.1 %all-to-all-done.6.totals_ref = f32[8,8,128]{2,1,0:T(8,128)S(1)} async-done(((f32[8,8,128]{2,1,0:T(8,128)}), f32[8,8,128]{2,1,0:T(8,128)S(1)}, u32[]{:S(2)}, u32[]{:S(2)}) %all-to-all-start.6) | async-done | bytes 32800 | tf_op jit(solution)/shard_map/all_to_all | solution.py:387
  116.7 5.6 %update.1 = (f32[64,256]{1,0:T(8,128)}, f32[64,256]{1,0:T(8,128)}, bf16[4096,256]{1,0:T(8,128)(2,1)}, f32[32,512]{1,0:T(8,128)}, f32[32,512]{1,0:T(8,128)}, /*index=5*/bf16[2048,512]{1,0:T(8,128)(2,1)}) custom-call(s32[1]{0:T(128)} %bitcast.1.row_ref, f32[8,8,128]{2,1,0:T(8,128)S(1)} %all-to-all-done.6.totals_ref, ...), custom_call_target="tpu_custom_call" | custom-call | flops 1073741824 | bytes 8388608 | tf_op jit(solution)/shard_map/update/pallas_call | solution.py:293
  (22 shorter events, 0.2 us)
Async XLA Ops:
  7.2 39.4 %copy-start = (bf16[512,512]{1,0:T(8,128)(2,1)S(1)}, bf16[512,512]{1,0:T(8,128)(2,1)}, u32[]{:S(2)}) copy-start(bf16[512,512]{1,0:T(8,128)(2,1)} %param.15) | copy-start | bytes 1572868
  8.8 10.5 %all-to-all-start = ((bf16[4,128,256]{2,1,0:T(8,128)(2,1)}), bf16[4,128,256]{2,1,0:T(8,128)(2,1)S(1)}, u32[]{:S(2)}, u32[]{:S(2)}) async-start(bf16[4,128,256]{2,1,0:T(8,128)(2,1)} %pack.1), calls=%async_computation | async-start | bytes 524288 | tf_op jit(solution)/shard_map/all_to_all | solution.py:353
  13.8 102.8 %all-gather.3.cloned.1.call-start = ((), (), s32[]{:S(2)}) async-start(), calls=%async_computation.7 | async-start | bytes 4456448 | tf_op jit(solution)/shard_map/all_gather | solution.py:359
  13.8 32.5 %copy-start.9 = (bf16[512,256]{1,0:T(8,128)(2,1)S(1)}, bf16[512,256]{1,0:T(8,128)(2,1)}, u32[]{:S(2)}) copy-start(bf16[512,256]{1,0:T(8,128)(2,1)} %param.13) | copy-start | bytes 786436
  19.4 0.7 copy-start.8
  46.5 56.0 %copy-start.2 = (f32[128,512]{1,0:T(8,128)S(1)}, f32[128,512]{1,0:T(8,128)}, u32[]{:S(2)}) copy-start(f32[128,512]{1,0:T(8,128)} %output_moment_ref.1) | copy-start | bytes 786436
  46.6 56.0 %copy-start.3 = (f32[128,512]{1,0:T(8,128)S(1)}, f32[128,512]{1,0:T(8,128)}, u32[]{:S(2)}) copy-start(f32[128,512]{1,0:T(8,128)} %output_second_ref.1) | copy-start | bytes 786436
  46.6 56.0 %copy-start.4 = (f32[128,256]{1,0:T(8,128)S(1)}, f32[128,256]{1,0:T(8,128)}, u32[]{:S(2)}) copy-start(f32[128,256]{1,0:T(8,128)} %value_moment_ref.1) | copy-start | bytes 393220
  46.6 56.0 %copy-start.5 = (f32[128,256]{1,0:T(8,128)S(1)}, f32[128,256]{1,0:T(8,128)}, u32[]{:S(2)}) copy-start(f32[128,256]{1,0:T(8,128)} %value_second_ref.1) | copy-start | bytes 393220
  64.6 21.5 %collective-permute-start = (f32[8,768]{1,0:T(8,128)S(1)}, f32[8,768]{1,0:T(8,128)S(1)}, u32[]{:S(2)}, u32[]{:S(2)}) collective-permute-start(f32[8,768]{1,0:T(8,128)S(1)} %reduce_sum.32), channel_id=1, source_target_pairs={{0,256},{128,384},{256,0},{384,128},{1,257},{129,385},{257,1},{385... | collective-permute-start | bytes 73736 | tf_op jit(solution)/shard_map/ppermute | solution.py:33
  76.9 9.2 %collective-permute-start.1 = (f32[8,768]{1,0:T(8,128)S(1)}, f32[8,768]{1,0:T(8,128)S(1)}, u32[]{:S(2)}, u32[]{:S(2)}) collective-permute-start(f32[8,768]{1,0:T(8,128)S(1)} %reduce_sum.32), channel_id=1, source_target_pairs={{0,128},{128,256},{256,384},{384,0},{1,129},{129,257},{257,385},{3... | collective-permute-start | bytes 73736 | tf_op jit(solution)/shard_map/ppermute | solution.py:33
  81.2 9.1 %collective-permute-start.2 = (f32[8,768]{1,0:T(8,128)S(1)}, f32[8,768]{1,0:T(8,128)S(1)}, u32[]{:S(2)}, u32[]{:S(2)}) collective-permute-start(f32[8,768]{1,0:T(8,128)S(1)} %reduce_sum.32), channel_id=1, source_target_pairs={{0,384},{128,0},{256,128},{384,256},{1,385},{129,1},{257,129},{385... | collective-permute-start | bytes 73736 | tf_op jit(solution)/shard_map/ppermute | solution.py:33
  90.3 26.4 %copy-start.1 = (bf16[2048,128]{1,0:T(8,128)(2,1)S(1)}, bf16[2048,128]{1,0:T(8,128)(2,1)}, u32[]{:S(2)}) copy-start(bf16[2048,128]{1,0:T(8,128)(2,1)} %output_factor_ref.1) | copy-start | bytes 1572868
  90.3 26.4 %copy-start.6 = (f32[64,256]{1,0:T(8,128)S(1)}, f32[64,256]{1,0:T(8,128)}, u32[]{:S(2)}) copy-start(f32[64,256]{1,0:T(8,128)} %value_master_ref.1) | copy-start | bytes 196612
  90.3 26.4 %copy-start.7 = (f32[32,512]{1,0:T(8,128)S(1)}, f32[32,512]{1,0:T(8,128)}, u32[]{:S(2)}) copy-start(f32[32,512]{1,0:T(8,128)} %output_master_ref.1) | copy-start | bytes 196612
  103.5 13.2 %all-to-all-start.6 = ((f32[8,8,128]{2,1,0:T(8,128)}), f32[8,8,128]{2,1,0:T(8,128)S(1)}, u32[]{:S(2)}, u32[]{:S(2)}) async-start(f32[8,8,128]{2,1,0:T(8,128)} %get-tuple-element.23), calls=%async_computation.6 | async-start | bytes 65536 | tf_op jit(solution)/shard_map/all_to_all | solution.py:387
Sparse Core Ops, SparseCore 0:
  20.2 78.1 all-gather.2

commit v4 on v3

--- a/solution.py
+++ b/solution.py
@@ -28,12 +28,9 @@
 
 def summed_far(part, axis):
     size = lax.axis_size(axis)
-
-    def shifted(by):
-        return lax.ppermute(part, axis, [(i, (i + by) % size) for i in range(size)])
-
-    opposite, before, after = shifted(2), shifted(1), shifted(3)
-    return (part + opposite) + (before + after)
+    for by in (size // 2, 1):
+        part = part + lax.ppermute(part, axis, [(i, i ^ by) for i in range(size)])
+    return part
 
 
 def contract_rows(left, right):
@@ -161,10 +158,10 @@
     row_ref,
     totals_ref,
     norm_ref,
-    value_factor_ref,
     output_factor_ref,
     value_master_ref,
     output_master_ref,
+    value_factor_hbm,
     masters_hbm,
     value_step_hbm,
     value_new_hbm,
@@ -173,6 +170,8 @@
     output_new_hbm,
     output_copy_hbm,
     masters,
+    value_factor,
+    value_here,
     value_copy,
     output_copy,
     value_step,
@@ -182,6 +181,8 @@
     value_pair,
     output_pair,
     in_sems,
+    factor_sems,
+    here_sem,
     value_sems,
     output_sems,
     own_sems,
@@ -210,7 +211,16 @@
             output_copy.at[rows], output_copy_hbm.at[rows], output_sems.at[k]
         )
 
+    def arriving_factor(k):
+        rows = pl.ds(k * group * value_rows, group * value_rows)
+        return pltpu.make_async_copy(value_factor_hbm.at[rows], value_factor.at[rows], factor_sems.at[k])
+
+    row = row_ref[0]
+    rows_here = pl.ds(pl.multiple_of(row * value_rows, value_rows), value_rows)
+    here = pltpu.make_async_copy(value_factor_hbm.at[rows_here], value_here, here_sem)
+    here.start()
     for k in range(chunks):
+        arriving_factor(k).start()
         arriving(k).start()
 
     totals = jnp.sum(totals_ref[...], axis=0)
@@ -225,9 +235,8 @@
         pair[:R, :] = high
         pair[R:, :] = (scaled - high.astype(jnp.float32)).astype(jnp.bfloat16)
 
-    row = row_ref[0]
-    value_here = value_factor_ref[pl.ds(pl.multiple_of(row * value_rows, value_rows), value_rows), :]
-    change = product(value_here, value_pair)
+    here.wait()
+    change = product(value_here[...], value_pair)
     value_step[...] = change * (-1.0 / STEP_RATE)
     value_new[...] = value_master_ref[...] + change
     output_here = output_factor_ref[
@@ -246,11 +255,12 @@
         copy.start()
 
     for k in range(chunks):
+        arriving_factor(k).wait()
         arriving(k).wait()
         count = group * value_rows
         rows = slice(k * count, (k + 1) * count)
         mine = slice(k * group, (k + 1) * group)
-        change = product(value_factor_ref[rows, :], value_pair)
+        change = product(value_factor[rows, :], value_pair)
         old = masters[mine, :value_rows, :].reshape(count, width)
         value_copy[rows, :] = (old.astype(jnp.float32) + change).astype(jnp.bfloat16)
         leaving_value(k).start()
@@ -292,11 +302,13 @@
     ]
     return pl.pallas_call(
         update_kernel,
-        in_specs=[pl.BlockSpec(memory_space=pltpu.SMEM)] + [in_vmem] * 6 + [anywhere],
+        in_specs=[pl.BlockSpec(memory_space=pltpu.SMEM)] + [in_vmem] * 5 + [anywhere] * 2,
         out_specs=[anywhere] * 6,
         out_shape=outs,
         scratch_shapes=[
             pltpu.VMEM(masters.shape, jnp.bfloat16),
+            pltpu.VMEM(value_factor.shape, jnp.bfloat16),
+            pltpu.VMEM((value_rows, R), jnp.bfloat16),
             pltpu.VMEM(outs[2].shape, jnp.bfloat16),
             pltpu.VMEM(outs[5].shape, jnp.bfloat16),
             pltpu.VMEM(value_master.shape, jnp.float32),
@@ -306,6 +318,8 @@
             pltpu.VMEM((2 * R, value_cols), jnp.bfloat16),
             pltpu.VMEM((2 * R, output_cols), jnp.bfloat16),
             pltpu.SemaphoreType.DMA((chunks,)),
+            pltpu.SemaphoreType.DMA((chunks,)),
+            pltpu.SemaphoreType.DMA,
             pltpu.SemaphoreType.DMA((chunks,)),
             pltpu.SemaphoreType.DMA((chunks,)),
             pltpu.SemaphoreType.DMA((4,)),
@@ -321,10 +335,10 @@
         row_index,
         totals,
         norm,
-        value_factor,
         output_factor,
         value_master,
         output_master,
+        value_factor,
         masters,
     )
 

time: 130 us -> 129 us (level)
    ppermute x3 -> x2, starting transfers between devices: 21.5 us -> 20.3 us  [summed_far(): part = part + lax.ppermute(part, axis, [(i, i ^ by) for i in range(size)])]
    ppermute x3 -> x2, waiting for transfers between devices: 4.11 us -> 2.99 us  [summed_far(): part = part + lax.ppermute(part, axis, [(i, i ^ by) for i in range(size)])]
  transfers between devices with their start and end apart: 6 -> 5, of which waited for: 3 -> 4; matrix products, arithmetic and copies ran while one was open for 2% -> 2% of each run, Pallas kernels for 2% -> 3%
where the time goes in v4:
time: 129 us; the launch traced here: 128 us
  blocking collectives  57.3 us (44%)
  starting transfers between devices  34 us (26%)
  between operations  14.2 us (11%)
  Pallas kernels  10.3 us (8%)
  waiting for transfers between devices  9.36 us (7%)
  other arithmetic  1.76 us (1%)
    all_to_all x2, blocking collectives, sent_to_all(): return lax.all_to_all(copies, axis, split_axis=0, concat_axis=0, tiled=True)  23.5 us
    ppermute x2, starting transfers between devices, summed_far(): part = part + lax.ppermute(part, axis, [(i, i ^ by) for i in range(size)])  20.3 us
    all_to_all x1, blocking collectives, per_device(): lax.all_to_all(partial, 'tp', split_axis=0, concat_axis=0, tiled=True)  16.2 us
    all_to_all x1, blocking collectives, per_device(): lax.all_to_all(gradient, 'y', split_axis=0, concat_axis=0, tiled=True)  9.58 us
    all_to_all x1, starting transfers between devices, per_device(): lax.all_to_all(totals, 'tp', split_axis=0, concat_axis=0, tiled=True)  8.68 us
    all_to_all x1, blocking collectives, per_device(): lax.all_to_all(gradient, 'zl', split_axis=0, concat_axis=0, tiled=True)  8.11 us
    pallas_call x1, Pallas kernels, updated(): pl.pallas_call(update_kernel, in_specs=[pl.BlockSpec(memory_space=pltpu.S...  5.38 us
    all_to_all x1, starting transfers between devices, per_device(): plane = lax.all_to_all(packed, 'y', split_axis=0, concat_axis=0, tiled=True)  5 us
  transfers between devices with their start and end apart: 5, of which 4 were waited for; matrix products, arithmetic and copies ran while one was open for 2% of the time, Pallas kernels for 3%

profile of v4, /device:TPU:1, one launch (start us, length us, event | category | flops | bytes accessed | tf_op | source)
XLA Modules:
  0.0 128.1 jit_solution(8087237635713540679)
XLA Ops:
  7.2 0.0 copy-start
  7.2 1.7 %pack.1 = bf16[4,128,256]{2,1,0:T(8,128)(2,1)} custom-call(f32[64,256]{1,0:T(8,128)} %value_master_ref.1, f32[32,512]{1,0:T(8,128)} %output_master_ref.1), custom_call_target="tpu_custom_call" | custom-call | tf_op jit(solution)/shard_map/pack/pallas_call | solution.py:65
  8.8 5.0 %all-to-all-start = ((bf16[4,128,256]{2,1,0:T(8,128)(2,1)}), bf16[4,128,256]{2,1,0:T(8,128)(2,1)S(1)}, u32[]{:S(2)}, u32[]{:S(2)}) async-start(bf16[4,128,256]{2,1,0:T(8,128)(2,1)} %pack.1), calls=%async_computation | async-start | bytes 524288 | tf_op jit(solution)/shard_map/all_to_all | solution.py:367
  13.8 2.3 %project.1 = bf16[8,64,256]{2,1,0:T(8,128)(2,1)} custom-call(s32[1]{0:T(128)} %bitcast.index_ref, bf16[512,512]{1,0:T(8,128)(2,1)} %input_ref.1, bf16[512,256]{1,0:T(8,128)(2,1)} %mixer_ref.1, bf16[4096,128]{1,0:T(8,128)(2,1)} %value_factor_hbm.1, bf16[2048,128]{1,0:T(8,128)(2,1)} %output_factor_ref.1), custom_call_target="tpu_custom_call" | custom-call | flops 100663296 | bytes 1048576 | tf_op jit(solution)/shard_map/project/pallas_call | solution.py:83
  16.1 3.3 %all-to-all-done = bf16[4,128,256]{2,1,0:T(8,128)(2,1)S(1)} async-done(((bf16[4,128,256]{2,1,0:T(8,128)(2,1)}), bf16[4,128,256]{2,1,0:T(8,128)(2,1)S(1)}, u32[]{:S(2)}, u32[]{:S(2)}) %all-to-all-start) | async-done | bytes 262176 | tf_op jit(solution)/shard_map/all_to_all | solution.py:367
  19.4 0.7 copy-done.8
  20.1 0.0 all-gather.3.cloned.1.call-update
  20.1 16.2 %all_to_all.35 = bf16[8,64,256]{2,1,0:T(8,128)(2,1)S(1)} all-to-all(bf16[8,64,256]{2,1,0:T(8,128)(2,1)} %project.1), channel_id=1, replica_groups=mesh['zh'=4,'zl'=4,'y'=4,'tp'=8] {'tp'}, dimensions={0} | all-to-all | bytes 524288 | tf_op jit(solution)/shard_map/all_to_all | solution.py:374
  36.3 10.0 %all_to_all.36 = bf16[8,64,256]{2,1,0:T(8,128)(2,1)S(1)} all-to-all(bf16[8,64,256]{2,1,0:T(8,128)(2,1)S(1)} %broadcast_in_dim.6), channel_id=1, replica_groups=mesh['zh'=4,'zl'=4,'y'=4,'tp'=8] {'tp'}, dimensions={0} | all-to-all | bytes 524288 | tf_op jit(solution)/shard_map/all_to_all | solution.py:26
  46.3 0.0 copy-done.9
  46.3 0.2 fusion.4
  46.5 0.0 copy-start.2
  46.6 0.0 copy-start.3
  46.6 0.0 copy-start.4
  46.6 0.0 copy-start.5
  46.6 0.2 fusion.2
  46.9 9.6 %all_to_all.37 = f32[4,32,768]{2,1,0:T(8,128)S(1)} all-to-all(f32[4,32,768]{2,1,0:T(8,128)S(1)} %bitcast.10), channel_id=1, replica_groups=mesh['zh'=4,'zl'=4,'y'=4,'tp'=8] {'y'}, dimensions={0} | all-to-all | bytes 786432 | tf_op jit(solution)/shard_map/all_to_all | solution.py:383
  56.5 8.1 %all_to_all.38 = f32[4,8,768]{2,1,0:T(8,128)S(1)} all-to-all(f32[4,8,768]{2,1,0:T(8,128)S(1)} %bitcast.13), channel_id=1, replica_groups=mesh['zh'=4,'zl'=4,'y'=4,'tp'=8] {'zl'}, dimensions={0} | all-to-all | bytes 196608 | tf_op jit(solution)/shard_map/all_to_all | solution.py:385
  64.6 12.3 %collective-permute-start = (f32[8,768]{1,0:T(8,128)S(1)}, f32[8,768]{1,0:T(8,128)S(1)}, u32[]{:S(2)}, u32[]{:S(2)}) collective-permute-start(f32[8,768]{1,0:T(8,128)S(1)} %reduce_sum.32), channel_id=1, source_target_pairs={{0,256},{128,384},{256,0},{384,128},{1,257},{129,385},{257,1},{385... | collective-permute-start | bytes 73736 | tf_op jit(solution)/shard_map/ppermute | solution.py:32
  76.9 1.7 %collective-permute-done = f32[8,768]{1,0:T(8,128)S(1)} collective-permute-done((f32[8,768]{1,0:T(8,128)S(1)}, f32[8,768]{1,0:T(8,128)S(1)}, u32[]{:S(2)}, u32[]{:S(2)}) %collective-permute-start) | collective-permute-done | bytes 24608 | tf_op jit(solution)/shard_map/ppermute | solution.py:32
  78.6 8.0 %collective-permute-start.1 = (f32[8,768]{1,0:T(8,128)S(1)}, f32[8,768]{1,0:T(8,128)S(1)}, u32[]{:S(2)}, u32[]{:S(2)}) collective-permute-start(f32[8,768]{1,0:T(8,128)S(1)} %add.26), channel_id=1, source_target_pairs={{0,128},{128,0},{256,384},{384,256},{1,129},{129,1},{257,385},{385... | collective-permute-start | bytes 73736 | tf_op jit(solution)/shard_map/ppermute | solution.py:32
  86.6 1.3 %collective-permute-done.1 = f32[8,768]{1,0:T(8,128)S(1)} collective-permute-done((f32[8,768]{1,0:T(8,128)S(1)}, f32[8,768]{1,0:T(8,128)S(1)}, u32[]{:S(2)}, u32[]{:S(2)}) %collective-permute-start.1) | collective-permute-done | bytes 24608 | tf_op jit(solution)/shard_map/ppermute | solution.py:32
  87.9 0.0 copy-start.7
  87.9 13.5 %all_to_all.39.gradient_ref = bf16[16,8,768]{2,1,0:T(8,128)(2,1)S(1)} all-to-all(bf16[16,8,768]{2,1,0:T(8,128)(2,1)S(1)} %broadcast_in_dim.7), channel_id=1, replica_groups=mesh['zh'=4,'zl'=4,'y'=4,'tp'=8] {'y','zl'}, dimensions={0} | all-to-all | bytes 393216 | tf_op jit(solution)/shard_map/all_to_all | solution.py:26
  101.4 0.0 copy-done.4
  101.4 0.0 copy-done.5
  101.5 1.0 norms.1
  102.4 8.7 %all-to-all-start.6 = ((f32[8,8,128]{2,1,0:T(8,128)}), f32[8,8,128]{2,1,0:T(8,128)S(1)}, u32[]{:S(2)}, u32[]{:S(2)}) async-start(f32[8,8,128]{2,1,0:T(8,128)} %get-tuple-element.23), calls=%async_computation.6 | async-start | bytes 65536 | tf_op jit(solution)/shard_map/all_to_all | solution.py:401
  111.1 0.9 fusion
  112.0 0.7 fusion.1
  112.7 3.1 %all-to-all-done.6.totals_ref = f32[8,8,128]{2,1,0:T(8,128)S(1)} async-done(((f32[8,8,128]{2,1,0:T(8,128)}), f32[8,8,128]{2,1,0:T(8,128)S(1)}, u32[]{:S(2)}, u32[]{:S(2)}) %all-to-all-start.6) | async-done | bytes 32800 | tf_op jit(solution)/shard_map/all_to_all | solution.py:401
  115.8 5.4 %update.1 = (f32[64,256]{1,0:T(8,128)}, f32[64,256]{1,0:T(8,128)}, bf16[4096,256]{1,0:T(8,128)(2,1)}, f32[32,512]{1,0:T(8,128)}, f32[32,512]{1,0:T(8,128)}, /*index=5*/bf16[2048,512]{1,0:T(8,128)(2,1)}) custom-call(s32[1]{0:T(128)} %bitcast.1.row_ref, f32[8,8,128]{2,1,0:T(8,128)S(1)} %all-to-all-done.6.totals_ref, ...), custom_call_target="tpu_custom_call" | custom-call | flops 1073741824 | bytes 8388608 | tf_op jit(solution)/shard_map/update/pallas_call | solution.py:303
  (21 shorter events, 0.2 us)
Async XLA Ops:
  7.2 39.4 %copy-start = (bf16[512,512]{1,0:T(8,128)(2,1)S(1)}, bf16[512,512]{1,0:T(8,128)(2,1)}, u32[]{:S(2)}) copy-start(bf16[512,512]{1,0:T(8,128)(2,1)} %param.15) | copy-start | bytes 1572868
  8.8 10.5 %all-to-all-start = ((bf16[4,128,256]{2,1,0:T(8,128)(2,1)}), bf16[4,128,256]{2,1,0:T(8,128)(2,1)S(1)}, u32[]{:S(2)}, u32[]{:S(2)}) async-start(bf16[4,128,256]{2,1,0:T(8,128)(2,1)} %pack.1), calls=%async_computation | async-start | bytes 524288 | tf_op jit(solution)/shard_map/all_to_all | solution.py:367
  13.8 102.0 %all-gather.3.cloned.1.call-start = ((), (), s32[]{:S(2)}) async-start(), calls=%async_computation.7 | async-start | bytes 4456448 | tf_op jit(solution)/shard_map/all_gather | solution.py:373
  13.8 32.5 %copy-start.9 = (bf16[512,256]{1,0:T(8,128)(2,1)S(1)}, bf16[512,256]{1,0:T(8,128)(2,1)}, u32[]{:S(2)}) copy-start(bf16[512,256]{1,0:T(8,128)(2,1)} %param.13) | copy-start | bytes 786436
  19.4 0.7 copy-start.8
  46.5 54.9 %copy-start.2 = (f32[128,512]{1,0:T(8,128)S(1)}, f32[128,512]{1,0:T(8,128)}, u32[]{:S(2)}) copy-start(f32[128,512]{1,0:T(8,128)} %output_moment_ref.1) | copy-start | bytes 786436
  46.6 54.9 %copy-start.3 = (f32[128,512]{1,0:T(8,128)S(1)}, f32[128,512]{1,0:T(8,128)}, u32[]{:S(2)}) copy-start(f32[128,512]{1,0:T(8,128)} %output_second_ref.1) | copy-start | bytes 786436
  46.6 54.9 %copy-start.4 = (f32[128,256]{1,0:T(8,128)S(1)}, f32[128,256]{1,0:T(8,128)}, u32[]{:S(2)}) copy-start(f32[128,256]{1,0:T(8,128)} %value_moment_ref.1) | copy-start | bytes 393220
  46.6 54.9 %copy-start.5 = (f32[128,256]{1,0:T(8,128)S(1)}, f32[128,256]{1,0:T(8,128)}, u32[]{:S(2)}) copy-start(f32[128,256]{1,0:T(8,128)} %value_second_ref.1) | copy-start | bytes 393220
  64.6 14.0 %collective-permute-start = (f32[8,768]{1,0:T(8,128)S(1)}, f32[8,768]{1,0:T(8,128)S(1)}, u32[]{:S(2)}, u32[]{:S(2)}) collective-permute-start(f32[8,768]{1,0:T(8,128)S(1)} %reduce_sum.32), channel_id=1, source_target_pairs={{0,256},{128,384},{256,0},{384,128},{1,257},{129,385},{257,1},{385... | collective-permute-start | bytes 73736 | tf_op jit(solution)/shard_map/ppermute | solution.py:32
  78.6 9.3 %collective-permute-start.1 = (f32[8,768]{1,0:T(8,128)S(1)}, f32[8,768]{1,0:T(8,128)S(1)}, u32[]{:S(2)}, u32[]{:S(2)}) collective-permute-start(f32[8,768]{1,0:T(8,128)S(1)} %add.26), channel_id=1, source_target_pairs={{0,128},{128,0},{256,384},{384,256},{1,129},{129,1},{257,385},{385... | collective-permute-start | bytes 73736 | tf_op jit(solution)/shard_map/ppermute | solution.py:32
  87.9 27.9 %copy-start.1 = (bf16[2048,128]{1,0:T(8,128)(2,1)S(1)}, bf16[2048,128]{1,0:T(8,128)(2,1)}, u32[]{:S(2)}) copy-start(bf16[2048,128]{1,0:T(8,128)(2,1)} %output_factor_ref.1) | copy-start | bytes 1572868
  87.9 27.9 %copy-start.6 = (f32[64,256]{1,0:T(8,128)S(1)}, f32[64,256]{1,0:T(8,128)}, u32[]{:S(2)}) copy-start(f32[64,256]{1,0:T(8,128)} %value_master_ref.1) | copy-start | bytes 196612
  87.9 27.9 %copy-start.7 = (f32[32,512]{1,0:T(8,128)S(1)}, f32[32,512]{1,0:T(8,128)}, u32[]{:S(2)}) copy-start(f32[32,512]{1,0:T(8,128)} %output_master_ref.1) | copy-start | bytes 196612
  102.4 13.4 %all-to-all-start.6 = ((f32[8,8,128]{2,1,0:T(8,128)}), f32[8,8,128]{2,1,0:T(8,128)S(1)}, u32[]{:S(2)}, u32[]{:S(2)}) async-start(f32[8,8,128]{2,1,0:T(8,128)} %get-tuple-element.23), calls=%async_computation.6 | async-start | bytes 65536 | tf_op jit(solution)/shard_map/all_to_all | solution.py:401
Sparse Core Ops, SparseCore 0:
  20.2 76.3 all-gather.2

commit v5 on v4

--- a/solution.py
+++ b/solution.py
@@ -152,6 +152,12 @@
     return jnp.dot(
         jnp.concatenate([rows, rows], axis=1), pair_ref[...], preferred_element_type=jnp.float32
     )
+
+
+def chunked(count):
+    part = count // 8
+    sizes = [part, 2 * part, 2 * part, 2 * part, count - 7 * part]
+    return [sum(sizes[:k]) for k in range(len(sizes))], sizes
 
 
 def update_kernel(
@@ -187,14 +193,14 @@
     output_sems,
     own_sems,
 ):
-    chunks = in_sems.shape[0]
     n_fs, _, width = masters.shape
-    group = n_fs // chunks
+    starts, sizes = chunked(n_fs)
+    chunks = len(sizes)
     value_rows, value_cols = value_master_ref.shape
     output_rows = output_master_ref.shape[0]
 
     def block(k):
-        return pl.ds(k * group, group)
+        return pl.ds(starts[k], sizes[k])
 
     def arriving(k):
         return pltpu.make_async_copy(
@@ -202,17 +208,17 @@
         )
 
     def leaving_value(k):
-        rows = pl.ds(k * group * value_rows, group * value_rows)
+        rows = pl.ds(starts[k] * value_rows, sizes[k] * value_rows)
         return pltpu.make_async_copy(value_copy.at[rows], value_copy_hbm.at[rows], value_sems.at[k])
 
     def leaving_output(k):
-        rows = pl.ds(k * group * output_rows, group * output_rows)
+        rows = pl.ds(starts[k] * output_rows, sizes[k] * output_rows)
         return pltpu.make_async_copy(
             output_copy.at[rows], output_copy_hbm.at[rows], output_sems.at[k]
         )
 
     def arriving_factor(k):
-        rows = pl.ds(k * group * value_rows, group * value_rows)
+        rows = pl.ds(starts[k] * value_rows, sizes[k] * value_rows)
         return pltpu.make_async_copy(value_factor_hbm.at[rows], value_factor.at[rows], factor_sems.at[k])
 
     row = row_ref[0]
@@ -257,15 +263,15 @@
     for k in range(chunks):
         arriving_factor(k).wait()
         arriving(k).wait()
-        count = group * value_rows
-        rows = slice(k * count, (k + 1) * count)
-        mine = slice(k * group, (k + 1) * group)
+        count = sizes[k] * value_rows
+        rows = slice(starts[k] * value_rows, starts[k] * value_rows + count)
+        mine = slice(starts[k], starts[k] + sizes[k])
         change = product(value_factor[rows, :], value_pair)
         old = masters[mine, :value_rows, :].reshape(count, width)
         value_copy[rows, :] = (old.astype(jnp.float32) + change).astype(jnp.bfloat16)
         leaving_value(k).start()
-        count = group * output_rows
-        rows = slice(k * count, (k + 1) * count)
+        count = sizes[k] * output_rows
+        rows = slice(starts[k] * output_rows, starts[k] * output_rows + count)
         change = product(output_factor_ref[rows, :], output_pair)
         for side in range(2):
             first = value_rows + side * output_rows
@@ -287,7 +293,7 @@
     row_index, totals, masters, value_factor, output_factor, norm, value_master, output_master
 ):
     n_fs, packed_rows, width = masters.shape
-    chunks = 4
+    chunks = len(chunked(n_fs)[1])
     value_rows, value_cols = value_master.shape
     output_rows, output_cols = output_master.shape
     in_vmem = pl.BlockSpec(memory_space=pltpu.VMEM)

time: 129 us -> 129 us (level)
  no operation moved by 1% of the time
where the time goes in v5:
time: 129 us; the launch traced here: 128 us
  blocking collectives  57.3 us (44%)
  starting transfers between devices  34 us (26%)
  between operations  14.2 us (11%)
  Pallas kernels  10.3 us (8%)
  waiting for transfers between devices  9.36 us (7%)
  other arithmetic  1.76 us (1%)
    all_to_all x2, blocking collectives, sent_to_all(): return lax.all_to_all(copies, axis, split_axis=0, concat_axis=0, tiled=True)  23.5 us
    ppermute x2, starting transfers between devices, summed_far(): part = part + lax.ppermute(part, axis, [(i, i ^ by) for i in range(size)])  20.3 us
    all_to_all x1, blocking collectives, per_device(): lax.all_to_all(partial, 'tp', split_axis=0, concat_axis=0, tiled=True)  16.2 us
    all_to_all x1, blocking collectives, per_device(): lax.all_to_all(gradient, 'y', split_axis=0, concat_axis=0, tiled=True)  9.58 us
    all_to_all x1, starting transfers between devices, per_device(): lax.all_to_all(totals, 'tp', split_axis=0, concat_axis=0, tiled=True)  8.68 us
    all_to_all x1, blocking collectives, per_device(): lax.all_to_all(gradient, 'zl', split_axis=0, concat_axis=0, tiled=True)  8.11 us
    pallas_call x1, Pallas kernels, updated(): pl.pallas_call(update_kernel, in_specs=[pl.BlockSpec(memory_space=pltpu.S...  5.43 us
    all_to_all x1, starting transfers between devices, per_device(): plane = lax.all_to_all(packed, 'y', split_axis=0, concat_axis=0, tiled=True)  5 us
  transfers between devices with their start and end apart: 5, of which 4 were waited for; matrix products, arithmetic and copies ran while one was open for 2% of the time, Pallas kernels for 3%

profile of v5, /device:TPU:1, one launch (start us, length us, event | category | flops | bytes accessed | tf_op | source)
XLA Modules:
  0.0 128.1 jit_solution(8539317924933750036)
XLA Ops:
  7.2 0.0 copy-start
  7.2 1.7 %pack.1 = bf16[4,128,256]{2,1,0:T(8,128)(2,1)} custom-call(f32[64,256]{1,0:T(8,128)} %value_master_ref.1, f32[32,512]{1,0:T(8,128)} %output_master_ref.1), custom_call_target="tpu_custom_call" | custom-call | tf_op jit(solution)/shard_map/pack/pallas_call | solution.py:65
  8.8 5.0 %all-to-all-start = ((bf16[4,128,256]{2,1,0:T(8,128)(2,1)}), bf16[4,128,256]{2,1,0:T(8,128)(2,1)S(1)}, u32[]{:S(2)}, u32[]{:S(2)}) async-start(bf16[4,128,256]{2,1,0:T(8,128)(2,1)} %pack.1), calls=%async_computation | async-start | bytes 524288 | tf_op jit(solution)/shard_map/all_to_all | solution.py:373
  13.8 0.0 all-gather.3.cloned.1.call-start
  13.8 2.3 %project.1 = bf16[8,64,256]{2,1,0:T(8,128)(2,1)} custom-call(s32[1]{0:T(128)} %bitcast.index_ref, bf16[512,512]{1,0:T(8,128)(2,1)} %input_ref.1, bf16[512,256]{1,0:T(8,128)(2,1)} %mixer_ref.1, bf16[4096,128]{1,0:T(8,128)(2,1)} %value_factor_hbm.1, bf16[2048,128]{1,0:T(8,128)(2,1)} %output_factor_ref.1), custom_call_target="tpu_custom_call" | custom-call | flops 100663296 | bytes 1048576 | tf_op jit(solution)/shard_map/project/pallas_call | solution.py:83
  16.1 3.3 %all-to-all-done = bf16[4,128,256]{2,1,0:T(8,128)(2,1)S(1)} async-done(((bf16[4,128,256]{2,1,0:T(8,128)(2,1)}), bf16[4,128,256]{2,1,0:T(8,128)(2,1)S(1)}, u32[]{:S(2)}, u32[]{:S(2)}) %all-to-all-start) | async-done | bytes 262176 | tf_op jit(solution)/shard_map/all_to_all | solution.py:373
  19.4 0.7 copy-done.8
  20.1 0.0 all-gather.3.cloned.1.call-update
  20.1 16.2 %all_to_all.35 = bf16[8,64,256]{2,1,0:T(8,128)(2,1)S(1)} all-to-all(bf16[8,64,256]{2,1,0:T(8,128)(2,1)} %project.1), channel_id=1, replica_groups=mesh['zh'=4,'zl'=4,'y'=4,'tp'=8] {'tp'}, dimensions={0} | all-to-all | bytes 524288 | tf_op jit(solution)/shard_map/all_to_all | solution.py:380
  36.3 10.0 %all_to_all.36 = bf16[8,64,256]{2,1,0:T(8,128)(2,1)S(1)} all-to-all(bf16[8,64,256]{2,1,0:T(8,128)(2,1)S(1)} %broadcast_in_dim.6), channel_id=1, replica_groups=mesh['zh'=4,'zl'=4,'y'=4,'tp'=8] {'tp'}, dimensions={0} | all-to-all | bytes 524288 | tf_op jit(solution)/shard_map/all_to_all | solution.py:26
  46.3 0.2 fusion.4
  46.5 0.0 copy-start.2
  46.6 0.0 copy-start.3
  46.6 0.0 copy-start.4
  46.6 0.0 copy-start.5
  46.6 0.2 fusion.2
  46.9 9.6 %all_to_all.37 = f32[4,32,768]{2,1,0:T(8,128)S(1)} all-to-all(f32[4,32,768]{2,1,0:T(8,128)S(1)} %bitcast.10), channel_id=1, replica_groups=mesh['zh'=4,'zl'=4,'y'=4,'tp'=8] {'y'}, dimensions={0} | all-to-all | bytes 786432 | tf_op jit(solution)/shard_map/all_to_all | solution.py:389
  56.5 8.1 %all_to_all.38 = f32[4,8,768]{2,1,0:T(8,128)S(1)} all-to-all(f32[4,8,768]{2,1,0:T(8,128)S(1)} %bitcast.13), channel_id=1, replica_groups=mesh['zh'=4,'zl'=4,'y'=4,'tp'=8] {'zl'}, dimensions={0} | all-to-all | bytes 196608 | tf_op jit(solution)/shard_map/all_to_all | solution.py:391
  64.6 12.3 %collective-permute-start = (f32[8,768]{1,0:T(8,128)S(1)}, f32[8,768]{1,0:T(8,128)S(1)}, u32[]{:S(2)}, u32[]{:S(2)}) collective-permute-start(f32[8,768]{1,0:T(8,128)S(1)} %reduce_sum.32), channel_id=1, source_target_pairs={{0,256},{128,384},{256,0},{384,128},{1,257},{129,385},{257,1},{385... | collective-permute-start | bytes 73736 | tf_op jit(solution)/shard_map/ppermute | solution.py:32
  76.9 1.7 %collective-permute-done = f32[8,768]{1,0:T(8,128)S(1)} collective-permute-done((f32[8,768]{1,0:T(8,128)S(1)}, f32[8,768]{1,0:T(8,128)S(1)}, u32[]{:S(2)}, u32[]{:S(2)}) %collective-permute-start) | collective-permute-done | bytes 24608 | tf_op jit(solution)/shard_map/ppermute | solution.py:32
  78.6 8.0 %collective-permute-start.1 = (f32[8,768]{1,0:T(8,128)S(1)}, f32[8,768]{1,0:T(8,128)S(1)}, u32[]{:S(2)}, u32[]{:S(2)}) collective-permute-start(f32[8,768]{1,0:T(8,128)S(1)} %add.26), channel_id=1, source_target_pairs={{0,128},{128,0},{256,384},{384,256},{1,129},{129,1},{257,385},{385... | collective-permute-start | bytes 73736 | tf_op jit(solution)/shard_map/ppermute | solution.py:32
  86.6 1.3 %collective-permute-done.1 = f32[8,768]{1,0:T(8,128)S(1)} collective-permute-done((f32[8,768]{1,0:T(8,128)S(1)}, f32[8,768]{1,0:T(8,128)S(1)}, u32[]{:S(2)}, u32[]{:S(2)}) %collective-permute-start.1) | collective-permute-done | bytes 24608 | tf_op jit(solution)/shard_map/ppermute | solution.py:32
  87.9 0.0 copy-start.7
  87.9 13.5 %all_to_all.39.gradient_ref = bf16[16,8,768]{2,1,0:T(8,128)(2,1)S(1)} all-to-all(bf16[16,8,768]{2,1,0:T(8,128)(2,1)S(1)} %broadcast_in_dim.7), channel_id=1, replica_groups=mesh['zh'=4,'zl'=4,'y'=4,'tp'=8] {'y','zl'}, dimensions={0} | all-to-all | bytes 393216 | tf_op jit(solution)/shard_map/all_to_all | solution.py:26
  101.4 0.0 copy-done.2
  101.5 1.0 norms.1
  102.4 8.7 %all-to-all-start.6 = ((f32[8,8,128]{2,1,0:T(8,128)}), f32[8,8,128]{2,1,0:T(8,128)S(1)}, u32[]{:S(2)}, u32[]{:S(2)}) async-start(f32[8,8,128]{2,1,0:T(8,128)} %get-tuple-element.23), calls=%async_computation.6 | async-start | bytes 65536 | tf_op jit(solution)/shard_map/all_to_all | solution.py:407
  111.1 0.9 fusion
  112.0 0.7 fusion.1
  112.7 3.1 %all-to-all-done.6.totals_ref = f32[8,8,128]{2,1,0:T(8,128)S(1)} async-done(((f32[8,8,128]{2,1,0:T(8,128)}), f32[8,8,128]{2,1,0:T(8,128)S(1)}, u32[]{:S(2)}, u32[]{:S(2)}) %all-to-all-start.6) | async-done | bytes 32800 | tf_op jit(solution)/shard_map/all_to_all | solution.py:407
  115.8 0.0 copy-done.1
  115.8 5.4 %update.1 = (f32[64,256]{1,0:T(8,128)}, f32[64,256]{1,0:T(8,128)}, bf16[4096,256]{1,0:T(8,128)(2,1)}, f32[32,512]{1,0:T(8,128)}, f32[32,512]{1,0:T(8,128)}, /*index=5*/bf16[2048,512]{1,0:T(8,128)(2,1)}) custom-call(s32[1]{0:T(128)} %bitcast.1.row_ref, f32[8,8,128]{2,1,0:T(8,128)S(1)} %all-to-all-done.6.totals_ref, ...), custom_call_target="tpu_custom_call" | custom-call | flops 1073741824 | bytes 8388608 | tf_op jit(solution)/shard_map/update/pallas_call | solution.py:309
  (21 shorter events, 0.2 us)
Async XLA Ops:
  7.2 39.4 %copy-start = (bf16[512,512]{1,0:T(8,128)(2,1)S(1)}, bf16[512,512]{1,0:T(8,128)(2,1)}, u32[]{:S(2)}) copy-start(bf16[512,512]{1,0:T(8,128)(2,1)} %param.15) | copy-start | bytes 1572868
  8.8 10.5 %all-to-all-start = ((bf16[4,128,256]{2,1,0:T(8,128)(2,1)}), bf16[4,128,256]{2,1,0:T(8,128)(2,1)S(1)}, u32[]{:S(2)}, u32[]{:S(2)}) async-start(bf16[4,128,256]{2,1,0:T(8,128)(2,1)} %pack.1), calls=%async_computation | async-start | bytes 524288 | tf_op jit(solution)/shard_map/all_to_all | solution.py:373
  13.8 102.0 %all-gather.3.cloned.1.call-start = ((), (), s32[]{:S(2)}) async-start(), calls=%async_computation.7 | async-start | bytes 4456448 | tf_op jit(solution)/shard_map/all_gather | solution.py:379
  13.8 32.5 %copy-start.9 = (bf16[512,256]{1,0:T(8,128)(2,1)S(1)}, bf16[512,256]{1,0:T(8,128)(2,1)}, u32[]{:S(2)}) copy-start(bf16[512,256]{1,0:T(8,128)(2,1)} %param.13) | copy-start | bytes 786436
  19.4 0.7 copy-start.8
  46.5 54.9 %copy-start.2 = (f32[128,512]{1,0:T(8,128)S(1)}, f32[128,512]{1,0:T(8,128)}, u32[]{:S(2)}) copy-start(f32[128,512]{1,0:T(8,128)} %output_moment_ref.1) | copy-start | bytes 786436
  46.6 54.9 %copy-start.3 = (f32[128,512]{1,0:T(8,128)S(1)}, f32[128,512]{1,0:T(8,128)}, u32[]{:S(2)}) copy-start(f32[128,512]{1,0:T(8,128)} %output_second_ref.1) | copy-start | bytes 786436
  46.6 54.9 %copy-start.4 = (f32[128,256]{1,0:T(8,128)S(1)}, f32[128,256]{1,0:T(8,128)}, u32[]{:S(2)}) copy-start(f32[128,256]{1,0:T(8,128)} %value_moment_ref.1) | copy-start | bytes 393220
  46.6 54.9 %copy-start.5 = (f32[128,256]{1,0:T(8,128)S(1)}, f32[128,256]{1,0:T(8,128)}, u32[]{:S(2)}) copy-start(f32[128,256]{1,0:T(8,128)} %value_second_ref.1) | copy-start | bytes 393220
  64.6 14.0 %collective-permute-start = (f32[8,768]{1,0:T(8,128)S(1)}, f32[8,768]{1,0:T(8,128)S(1)}, u32[]{:S(2)}, u32[]{:S(2)}) collective-permute-start(f32[8,768]{1,0:T(8,128)S(1)} %reduce_sum.32), channel_id=1, source_target_pairs={{0,256},{128,384},{256,0},{384,128},{1,257},{129,385},{257,1},{385... | collective-permute-start | bytes 73736 | tf_op jit(solution)/shard_map/ppermute | solution.py:32
  78.6 9.3 %collective-permute-start.1 = (f32[8,768]{1,0:T(8,128)S(1)}, f32[8,768]{1,0:T(8,128)S(1)}, u32[]{:S(2)}, u32[]{:S(2)}) collective-permute-start(f32[8,768]{1,0:T(8,128)S(1)} %add.26), channel_id=1, source_target_pairs={{0,128},{128,0},{256,384},{384,256},{1,129},{129,1},{257,385},{385... | collective-permute-start | bytes 73736 | tf_op jit(solution)/shard_map/ppermute | solution.py:32
  87.9 27.9 %copy-start.1 = (bf16[2048,128]{1,0:T(8,128)(2,1)S(1)}, bf16[2048,128]{1,0:T(8,128)(2,1)}, u32[]{:S(2)}) copy-start(bf16[2048,128]{1,0:T(8,128)(2,1)} %output_factor_ref.1) | copy-start | bytes 1572868
  87.9 27.9 %copy-start.6 = (f32[64,256]{1,0:T(8,128)S(1)}, f32[64,256]{1,0:T(8,128)}, u32[]{:S(2)}) copy-start(f32[64,256]{1,0:T(8,128)} %value_master_ref.1) | copy-start | bytes 196612
  87.9 27.9 %copy-start.7 = (f32[32,512]{1,0:T(8,128)S(1)}, f32[32,512]{1,0:T(8,128)}, u32[]{:S(2)}) copy-start(f32[32,512]{1,0:T(8,128)} %output_master_ref.1) | copy-start | bytes 196612
  102.4 13.4 %all-to-all-start.6 = ((f32[8,8,128]{2,1,0:T(8,128)}), f32[8,8,128]{2,1,0:T(8,128)S(1)}, u32[]{:S(2)}, u32[]{:S(2)}) async-start(f32[8,8,128]{2,1,0:T(8,128)} %get-tuple-element.23), calls=%async_computation.6 | async-start | bytes 65536 | tf_op jit(solution)/shard_map/all_to_all | solution.py:407
Sparse Core Ops, SparseCore 0:
  20.2 76.3 all-gather.2
